TPU v7x, 32 devices: a whole 2x2x4 slice. The times are simulated.
32 devices in a mesh: rep: 2 (over x), fs: 8 (over z, y), tp: 2 (over core).
Axes of the slice: x: 2, y: 2, z: 4, core: 2. Of those that a mesh axis runs over, the one named last changes fastest.
Arguments:
- x_later: bfloat16 [2048, 2048], P(('rep', 'fs')), may hold values from -6 to 6
- kept_input_rows: bfloat16 [2048, 2048], P(('rep', 'fs')), may hold values from -6 to 6
- cotangent: bfloat16 [2048, 2048], P(('rep', 'fs')), may hold values from -8 to 8
- norm_gain_vector: float32 [2048], replicated, may hold values from 0.1 to 1.9
- up_weight: bfloat16 [2048, 4096], P('fs', 'tp'), may hold values from -0.125 to 0.125
- down_weight: bfloat16 [4096, 2048], P('tp', 'fs'), may hold values from -0.09375 to 0.09375
- up_sum: float32 [2048, 4096], P('fs', 'tp'), may hold values from -6 to 6
- down_sum: float32 [4096, 2048], P('tp', 'fs'), may hold values from -6 to 6
Outputs:
- mixed: bfloat16 [2048, 2048], P(('rep', 'fs'))
- input_gradient_rows: bfloat16 [2048, 2048], P(('rep', 'fs'))
- up_total: float32 [2048, 4096], P('fs', 'tp')
- down_total: float32 [4096, 2048], P('tp', 'fs')
All inputs are finite; a program needn't handle non-finite values.
Results may differ from a plain program's by a relative error of at most 0.018.
Values may be sent and summed in bfloat16 or wider, within the bound.
A program may use at most 128 MiB of HBM per device.

v0:
```python
import functools

import jax
import jax.numpy as jnp
from jax import lax
from jax.experimental import pallas as pl
from jax.experimental.pallas import tpu as pltpu
from jax.sharding import PartitionSpec as P

EPSILON = 1e-06
MESH = pl.DeviceIdType.MESH
TRANSPOSED = (((1,), (1,)), ((), ()))
LEADING = (((0,), (0,)), ((), ()))


def norm_partial_terms(values, norm_gain_vector):
    floats = values.astype(jnp.float32)
    inverse = lax.rsqrt(jnp.mean(floats * floats, axis=-1, keepdims=True) + EPSILON)
    unit_rows = floats * inverse
    normed = (unit_rows * norm_gain_vector).astype(jnp.bfloat16)
    return (inverse, unit_rows, normed)


def squared_relu(pre_act):
    return jnp.square(jax.nn.relu(pre_act)).astype(jnp.bfloat16)


def body(
    x_later, kept_input_rows, cotangent, norm_gain_vector, up_weight, down_weight, up_sum, down_sum
):
    row_count = x_later.shape[0]
    grad_scale = float(row_count * lax.axis_size("rep") * lax.axis_size("fs")) ** (-0.5)
    inv_later, unit_later, normed_later = norm_partial_terms(x_later, norm_gain_vector)
    inverse_rms_kept, unit_kept_rows, normed_kept_rows = norm_partial_terms(
        kept_input_rows, norm_gain_vector
    )
    stacked = jnp.concatenate([normed_kept_rows, normed_later], axis=0)
    up_whole = lax.all_gather(up_weight, "fs", axis=0, tiled=True)
    down_whole = lax.all_gather(down_weight, "fs", axis=1, tiled=True)
    pre_act = jnp.dot(stacked, up_whole, preferred_element_type=jnp.float32)
    pre_saved = pre_act[:row_count]
    hidden_saved = squared_relu(pre_saved)
    hidden_later = squared_relu(pre_act[row_count:])
    mixed_part = jnp.dot(hidden_later, down_whole, preferred_element_type=jnp.float32)
    hidden_grad = lax.dot_general(
        cotangent, down_whole, TRANSPOSED, preferred_element_type=jnp.float32
    )
    pre_grad = (hidden_grad * 2.0 * jax.nn.relu(pre_saved)).astype(jnp.bfloat16)
    back_part = lax.dot_general(pre_grad, up_whole, TRANSPOSED, preferred_element_type=jnp.float32)
    mixed_sum, back_sum = (
        lax.psum(mixed_part.astype(jnp.bfloat16), "tp").astype(jnp.float32),
        lax.psum(back_part.astype(jnp.bfloat16), "tp").astype(jnp.float32),
    )
    mixed = mixed_sum.astype(jnp.bfloat16)
    scaled_rows = back_sum * norm_gain_vector
    input_gradient_rows = (
        inverse_rms_kept
        * (
            scaled_rows
            - unit_kept_rows * jnp.mean(scaled_rows * unit_kept_rows, axis=-1, keepdims=True)
        )
    ).astype(jnp.bfloat16)
    cot_columns, normed_columns = (
        lax.all_to_all(cotangent, "fs", split_axis=1, concat_axis=0, tiled=True),
        lax.all_to_all(normed_kept_rows, "fs", split_axis=1, concat_axis=0, tiled=True),
    )
    columns = normed_columns
    up_grad = grad_scale * lax.dot_general(
        columns,
        lax.all_gather(pre_grad, "fs", axis=0, tiled=True),
        LEADING,
        preferred_element_type=jnp.float32,
    )
    columns = cot_columns
    down_grad = lax.dot_general(
        lax.all_gather(hidden_saved, "fs", axis=0, tiled=True),
        columns,
        LEADING,
        preferred_element_type=jnp.float32,
    )
    up_added, down_added = (
        lax.psum(up_grad.astype(jnp.bfloat16), "rep").astype(jnp.float32),
        lax.psum((down_grad * grad_scale).astype(jnp.bfloat16), "rep").astype(jnp.float32),
    )
    return (mixed, input_gradient_rows, up_sum + up_added, down_sum + down_added)


def swap(values, axis):
    size = lax.axis_size(axis)
    return lax.ppermute(values, axis, [(i, i ^ 1) for i in range(size)])


def own_half(values, axis_index, dim):
    return lax.dynamic_index_in_dim(values, axis_index, dim, keepdims=False)


def line_shift(values, shift):
    size = lax.axis_size("fs")
    outer = size // 2
    return lax.ppermute(
        values, "fs", [(i, ((i // 2 + shift) % outer) * 2 + i % 2) for i in range(size)]
    )


def ordered(first, second, axis_index):
    return jnp.where(axis_index == 0, jnp.stack([first, second]), jnp.stack([second, first]))


def scatter_tokens(partial, rows):
    width = partial.shape[1]
    outer = lax.axis_size("fs") // 2
    blocks = partial.reshape(2, 2, outer, rows // 2, width)
    got = swap(blocks[1], "tp")
    blocks = (blocks[0].astype(jnp.float32) + got.astype(jnp.float32)).astype(jnp.bfloat16)
    got = swap(blocks[1], "fs")
    blocks = (blocks[0].astype(jnp.float32) + got.astype(jnp.float32)).astype(jnp.bfloat16)
    place = lax.axis_index("fs") // 2
    total = own_half(blocks, place, 0).astype(jnp.float32)
    for s in range(1, outer):
        sent = own_half(blocks, (place + s) % outer, 0)
        total = total + line_shift(sent, s).astype(jnp.float32)
    half = total.astype(jnp.bfloat16)
    whole = ordered(half, swap(half, "tp"), lax.axis_index("tp"))
    return whole.reshape(rows, width).astype(jnp.float32)


def gather_kernel(
    n_fs, own, up, down, tok, up_out, down_out,
    line_send, line_recv, pair_send, pair_recv, core_send, core_recv,
    weight_send, weight_recv, local_sem,
):
    rep, fs, core = lax.axis_index("rep"), lax.axis_index("fs"), lax.axis_index("tp")
    outer = n_fs // 2
    place = fs // 2
    pair = fs % 2
    depth, units = up.shape
    own_units = units // n_fs
    part = own_units // 2
    other_pair = (rep, place * 2 + 1 - pair, core)
    other_core = (rep, fs, 1 - core)
    other_rep = (1 - rep, fs, core)

    barrier = pltpu.get_barrier_semaphore()
    peers = [other_core, other_rep]
    peers += [(rep, lax.rem(fs + k, n_fs), core) for k in range(1, n_fs)]
    for peer in peers:
        pl.semaphore_signal(barrier, inc=1, device_id=peer, device_id_type=MESH)
    pl.semaphore_wait(barrier, len(peers))

    def copy(source, target, send, recv, device):
        return pltpu.make_async_remote_copy(
            src_ref=source, dst_ref=target, send_sem=send, recv_sem=recv,
            device_id=device, device_id_type=MESH,
        )

    def slot(other, far, index):
        return tok.at[:, other, far, index]

    def to_line(source, index, way):
        step = 1 if way else -1
        target = (rep, fs + 2 * step, core)
        return copy(source, slot(0, 0, index), line_send.at[way, index], line_recv.at[index], target)

    def to_pair(source, index):
        return copy(
            source, slot(0, 1, index), pair_send.at[index], pair_recv.at[index], other_pair
        )

    def to_core(source, far, index):
        return copy(
            source, slot(1, far, index), core_send.at[far, index], core_recv.at[far, index],
            other_core,
        )

    def up_source(k):
        start = pl.multiple_of(k * own_units + rep * part, part)
        return up.at[:, pl.ds(start, part)]

    def down_source(k):
        start = pl.multiple_of(k * own_units + rep * part, part)
        return down.at[pl.ds(start, part), :]

    def up_slot(k, half):
        return up_out.at[k, :, half * part : (half + 1) * part]

    def down_slot(k, half):
        columns = pl.ds(pl.multiple_of(k * depth, depth), depth)
        return down_out.at[half * part : (half + 1) * part, columns]

    def up_copy(k):
        return copy(
            up_source(k), up_slot(fs, 0), weight_send.at[0, 0, k], weight_recv.at[0, 0, fs],
            (rep, k, core),
        )

    def down_copy(k):
        return copy(
            down_source(k), down_slot(fs, 0), weight_send.at[0, 1, k], weight_recv.at[0, 1, fs],
            (rep, k, core),
        )

    def up_pass(source, k):
        return copy(
            source, up_slot(k, 1), weight_send.at[1, 0, k], weight_recv.at[1, 0, k], other_rep
        )

    def down_pass(source, k):
        return copy(
            source, down_slot(k, 1), weight_send.at[1, 1, k], weight_recv.at[1, 1, k], other_rep
        )

    def landed(target, sem):
        copy(target, target, sem, sem, other_core).wait_recv()

    @pl.when(place > 0)
    def _():
        to_line(own, place, 0).start()

    @pl.when(place < outer - 1)
    def _():
        to_line(own, place, 1).start()

    to_pair(own, place).start()
    to_core(own, 0, place).start()
    keep = [
        pltpu.make_async_copy(own, slot(0, 0, place), local_sem.at[0]),
        pltpu.make_async_copy(up_source(fs), up_slot(fs, 0), local_sem.at[1]),
        pltpu.make_async_copy(down_source(fs), down_slot(fs, 0), local_sem.at[2]),
    ]
    for one in keep:
        one.start()
    up_pass(up_source(fs), fs).start()
    down_pass(down_source(fs), fs).start()
    for k in range(1, n_fs):
        peer = lax.rem(fs + k, n_fs)
        up_copy(peer).start()
        down_copy(peer).start()

    for d in range(1, outer):
        if d == outer - 1:
            for k in range(1, n_fs):
                peer = lax.rem(fs + n_fs - k, n_fs)
                landed(up_slot(peer, 0), weight_recv.at[0, 0, peer])
                up_pass(up_slot(peer, 0), peer).start()
                landed(down_slot(peer, 0), weight_recv.at[0, 1, peer])
                down_pass(down_slot(peer, 0), peer).start()
        for way in range(2):
            index = place - d if way else place + d
            there = index >= 0 if way else index < outer
            more = place < outer - 1 if way else place > 0

            @pl.when(there)
            def _(index=index, way=way, more=more):
                landed(slot(0, 0, index), line_recv.at[index])

                @pl.when(more)
                def _():
                    to_line(slot(0, 0, index), index, way).start()

                to_pair(slot(0, 0, index), index).start()
                to_core(slot(0, 0, index), 0, index).start()

    def pass_pair(index):
        landed(slot(0, 1, index), pair_recv.at[index])
        to_core(slot(0, 1, index), 1, index).start()

    pass_pair(place)
    for d in range(1, outer):
        for way in range(2):
            index = place - d if way else place + d

            @pl.when(index >= 0 if way else index < outer)
            def _(index=index):
                pass_pair(index)

    for one in keep:
        one.wait()
    for k in range(n_fs):
        landed(up_slot(k, 1), weight_recv.at[1, 0, k])
        landed(down_slot(k, 1), weight_recv.at[1, 1, k])
        up_pass(up_slot(k, 0), k).wait_send()
        down_pass(down_slot(k, 0), k).wait_send()
    for k in range(1, n_fs):
        peer = lax.rem(fs + k, n_fs)
        up_copy(peer).wait_send()
        down_copy(peer).wait_send()
    for index in range(outer):
        to_pair(own, index).wait_send()
        for far in range(2):
            landed(slot(1, far, index), core_recv.at[far, index])
            to_core(own, far, index).wait_send()

        @pl.when(jnp.logical_and(index >= place, place > 0))
        def _(index=index):
            to_line(own, index, 0).wait_send()

        @pl.when(jnp.logical_and(index <= place, place < outer - 1))
        def _(index=index):
            to_line(own, index, 1).wait_send()


def gather_all(blocks, up_weight, down_weight):
    n_fs = lax.axis_size("fs")
    outer = n_fs // 2
    arrays, rows, width = blocks.shape
    depth, units = up_weight.shape
    own_units = units // n_fs
    dma = pltpu.SemaphoreType.DMA
    tok, up_own, down_own = pl.pallas_call(
        functools.partial(gather_kernel, n_fs),
        out_shape=(
            jax.ShapeDtypeStruct((arrays, 2, 2, outer, rows, width), blocks.dtype),
            jax.ShapeDtypeStruct((n_fs, depth, own_units), up_weight.dtype),
            jax.ShapeDtypeStruct((own_units, n_fs * depth), down_weight.dtype),
        ),
        in_specs=[pl.BlockSpec(memory_space=pl.ANY)] * 3,
        out_specs=[pl.BlockSpec(memory_space=pl.ANY)] * 3,
        scratch_shapes=[
            dma((2, outer)), dma((outer,)), dma((outer,)), dma((outer,)),
            dma((2, outer)), dma((2, outer)), dma((2, 2, n_fs)), dma((2, 2, n_fs)), dma((3,)),
        ],
        compiler_params=pltpu.CompilerParams(collective_id=0, has_side_effects=True),
    )(blocks, up_weight, down_weight)
    return tok, up_own.reshape(n_fs * depth, own_units), down_own


def hidden_body(
    x_later, kept_input_rows, cotangent, norm_gain_vector, up_weight, down_weight, up_sum, down_sum
):
    row_count, width = x_later.shape
    n_fs = lax.axis_size("fs")
    grad_scale = float(row_count * lax.axis_size("rep") * n_fs) ** (-0.5)
    group = lax.axis_index("rep")
    depth, units = up_weight.shape
    own_units = units // n_fs
    inv_later, unit_later, normed_later = norm_partial_terms(x_later, norm_gain_vector)
    inverse_rms_kept, unit_kept_rows, normed_kept_rows = norm_partial_terms(
        kept_input_rows, norm_gain_vector
    )
    part = own_units // 2
    part = own_units // 2
    core = lax.axis_index("tp")
    blocks = jnp.stack(
        [
            own_half(values.reshape(2, row_count // 2, width), core, 0)
            for values in (normed_kept_rows, cotangent, normed_later)
        ]
    )
    tok, up_own, down_own = gather_all(blocks, up_weight, down_weight)
    normed_saved, cot, normed_next = (tok[i].reshape(-1, width) for i in range(3))

    pre_saved = jnp.dot(normed_saved, up_own, preferred_element_type=jnp.float32)
    hidden_saved = squared_relu(pre_saved)
    hidden_grad = lax.dot_general(cot, down_own, TRANSPOSED, preferred_element_type=jnp.float32)
    pre_grad = (hidden_grad * 2.0 * jax.nn.relu(pre_saved)).astype(jnp.bfloat16)
    up_grad = grad_scale * lax.dot_general(
        normed_saved, pre_grad, LEADING, preferred_element_type=jnp.float32
    )
    down_grad = grad_scale * lax.dot_general(
        hidden_saved, cot, LEADING, preferred_element_type=jnp.float32
    )
    up_got = swap(up_grad[:, part:].astype(jnp.bfloat16), "rep")
    down_got = swap(down_grad[part:].astype(jnp.bfloat16), "rep")
    back_part = lax.dot_general(pre_grad, up_own, TRANSPOSED, preferred_element_type=jnp.float32)
    hidden_later = squared_relu(
        jnp.dot(normed_next, up_own, preferred_element_type=jnp.float32)
    )
    mixed_part = jnp.dot(hidden_later, down_own, preferred_element_type=jnp.float32)
    up_half = (up_grad[:, :part] + up_got.astype(jnp.float32)).astype(jnp.bfloat16)
    down_half = (down_grad[:part] + down_got.astype(jnp.float32)).astype(jnp.bfloat16)
    up_half = lax.all_to_all(up_half.reshape(n_fs, depth, part), "fs", 0, 0, tiled=True)
    down_half = down_half.reshape(part, n_fs, depth).transpose(1, 0, 2)
    down_half = lax.all_to_all(down_half, "fs", 0, 0, tiled=True)
    up_added = ordered(up_half, swap(up_half, "rep"), group)
    up_added = up_added.transpose(2, 1, 0, 3).reshape(depth, units)
    down_added = ordered(down_half, swap(down_half, "rep"), group)
    down_added = down_added.transpose(1, 0, 2, 3).reshape(units, depth)

    back_sum = scatter_tokens(back_part.astype(jnp.bfloat16), row_count)
    mixed = scatter_tokens(mixed_part.astype(jnp.bfloat16), row_count).astype(jnp.bfloat16)
    scaled_rows = back_sum * norm_gain_vector
    input_gradient_rows = (
        inverse_rms_kept
        * (
            scaled_rows
            - unit_kept_rows * jnp.mean(scaled_rows * unit_kept_rows, axis=-1, keepdims=True)
        )
    ).astype(jnp.bfloat16)
    return (
        mixed,
        input_gradient_rows,
        up_sum + up_added.astype(jnp.float32),
        down_sum + down_added.astype(jnp.float32),
    )


def chosen_body(*args):
    units = args[4].shape[1]
    n_fs = lax.axis_size("fs")
    pairs = lax.axis_size("tp") == 2 and lax.axis_size("rep") == 2 and n_fs % 2 == 0
    return (hidden_body if pairs and units % (128 * n_fs) == 0 else body)(*args)


def solution(mesh):
    return jax.shard_map(
        chosen_body,
        mesh=mesh,
        in_specs=(
            P(("rep", "fs"), None),
            P(("rep", "fs"), None),
            P(("rep", "fs"), None),
            P(),
            P("fs", "tp"),
            P("tp", "fs"),
            P("fs", "tp"),
            P("tp", "fs"),
        ),
        out_specs=(P(("rep", "fs"), None), P(("rep", "fs"), None), P("fs", "tp"), P("tp", "fs")),
        check_vma=False,
    )
```

profile of v0, /device:TPU:0, one launch (start us, length us, event | category | flops | bytes accessed | tf_op | source)
XLA Modules:
  0.0 251.1 jit_solution(15297363154464158835)
XLA Ops:
  5.8 101.3 %shard_map.111 = (bf16[3,2,2,4,64,2048]{5,4,3,2,1,0:T(8,128)(2,1)}, bf16[8,256,256]{2,1,0:T(8,128)(2,1)}, bf16[256,2048]{1,0:T(8,128)(2,1)}) custom-call(bf16[3,64,2048]{2,1,0:T(8,128)(2,1)} %pad_maximum_fusion.own, bf16[256,2048]{1,0:T(8,128)(2,1)} %up.1, bf16[2048,256]{1,0:T(8,128)(2,1)} %down.1), custom_call_target="tpu_custom_call" | custom-call | tf_op jit(solution)/shard_map/pallas_call | solution.py:309
  107.1 7.2 %fusion.31 = (bf16[1,2,2,4,64,2048]{5,4,3,2,1,0:T(8,128)(2,1)S(1)}, bf16[1,2,2,4,64,2048]{5,4,3,2,1,0:T(8,128)(2,1)S(1)}, bf16[1,2,2,4,64,2048]{5,4,3,2,1,0:T(8,128)(2,1)}) fusion(bf16[3,2,2,4,64,2048]{5,4,3,2,1,0:T(8,128)(2,1)} %get-tuple-element.7), kind=kLoop, calls=%fused_computation.78 | loop fusion | bytes 25165824 | tf_op jit(solution)/shard_map/slice | solution.py:350
  126.3 5.5 %collective-permute-done.14 = bf16[128,2048]{1,0:T(8,128)(2,1)S(1)} collective-permute-done((bf16[128,2048]{1,0:T(8,128)(2,1)S(1)}, bf16[128,2048]{1,0:T(8,128)(2,1)S(1)}, u32[]{:S(2)}, u32[]{:S(2)}) %collective-permute-start.14) | collective-permute-done | bytes 524320 | tf_op jit(solution)/shard_map/ppermute | solution.py:90
  132.7 4.6 %all-to-all-start.1 = ((bf16[8,128,256]{2,1,0:T(8,128)(2,1)}), bf16[8,128,256]{2,1,0:T(8,128)(2,1)S(1)}, u32[]{:S(2)}, u32[]{:S(2)}) async-start(bf16[8,128,256]{2,1,0:T(8,128)(2,1)} %bitcast.83), calls=%async_computation.1 | async-start | bytes 1048576 | tf_op jit(solution)/shard_map/all_to_all | solution.py:373
  137.3 9.1 %convolution_convert_fusion.1 = bf16[1024,2048]{1,0:T(8,128)(2,1)} fusion(bf16[256,2048]{1,0:T(8,128)(2,1)} %get-tuple-element.9, bf16[1024,2048]{1,0:T(8,128)(2,1)} %bitcast.89, bf16[2048,256]{1,0:T(8,128)(2,1)} %bitcast.98), kind=kOutput, calls=%fused_computation.5 | convolution fusion | flops 2150367232 | bytes 10485760 | tf_op jit(solution)/shard_map/dot_general | solution.py:368
  146.4 2.3 fusion.21
  148.7 2.2 all-to-all-done.1
  150.9 3.8 %all-to-all-start = ((bf16[8,256,128]{2,1,0:T(8,128)(2,1)}), bf16[8,256,128]{2,1,0:T(8,128)(2,1)S(1)}, u32[]{:S(2)}, u32[]{:S(2)}) async-start(bf16[8,256,128]{2,1,0:T(8,128)(2,1)} %bitcast.94), calls=%async_computation | async-start | bytes 1048576 | tf_op jit(solution)/shard_map/all_to_all | solution.py:371
  154.7 4.8 %fusion.33 = (bf16[512,2048]{1,0:T(8,128)(2,1)}, bf16[512,2048]{1,0:T(8,128)(2,1)}) fusion(bf16[1024,2048]{1,0:T(8,128)(2,1)} %convolution_convert_fusion.1), kind=kLoop, calls=%fused_computation.80 | loop fusion | bytes 8388608 | tf_op jit(solution)/shard_map/slice | solution.py:113
  161.0 7.4 %all-to-all-done = bf16[8,256,128]{2,1,0:T(8,128)(2,1)S(1)} async-done(((bf16[8,256,128]{2,1,0:T(8,128)(2,1)}), bf16[8,256,128]{2,1,0:T(8,128)(2,1)S(1)}, u32[]{:S(2)}, u32[]{:S(2)}) %all-to-all-start) | async-done | bytes 524320 | tf_op jit(solution)/shard_map/all_to_all | solution.py:371
  169.9 4.5 %collective-permute-done.15 = bf16[8,128,256]{2,1,0:T(8,128)(2,1)} collective-permute-done((bf16[8,128,256]{2,1,0:T(8,128)(2,1)S(1)}, bf16[8,128,256]{2,1,0:T(8,128)(2,1)}, u32[]{:S(2)}, u32[]{:S(2)}) %collective-permute-start.15) | collective-permute-done | bytes 524320 | tf_op jit(solution)/shard_map/ppermute | solution.py:90
  175.8 2.4 fusion
  179.3 2.0 collective-permute-start.7
  181.3 2.4 fusion.1
  188.3 2.9 %copy.16 = f32[256,8,2,128]{3,2,1,0:T(2,128)} copy(f32[256,8,2,128]{3,0,1,2:T(8,128)S(1)} %convert_bitcast_fusion) | data formatting | bytes 4194304 | tf_op jit(solution)/shard_map/convert_element_type | solution.py:392
  191.2 3.9 %reshape.100 = f32[256,2048]{1,0:T(8,128)} reshape(f32[256,8,2,128]{3,2,1,0:T(2,128)} %copy.16) | data formatting | bytes 4194304 | tf_op jit(solution)/shard_map/convert_element_type | solution.py:392
  195.1 4.0 %add.131 = f32[256,2048]{1,0:T(8,128)} add(f32[256,2048]{1,0:T(8,128)} %param.14, f32[256,2048]{1,0:T(8,128)} %reshape.100) | non-fusion elementwise | flops 524288 | bytes 6291456 | tf_op jit(solution)/shard_map/add | solution.py:392
  199.1 6.5 %collective-permute-done.7 = bf16[4,64,2048]{2,1,0:T(8,128)(2,1)} collective-permute-done((bf16[4,64,2048]{2,1,0:T(8,128)(2,1)}, bf16[4,64,2048]{2,1,0:T(8,128)(2,1)}, u32[]{:S(2)}, u32[]{:S(2)}) %collective-permute-start.7) | collective-permute-done | bytes 1048608 | tf_op jit(solution)/shard_map/ppermute | solution.py:90
  207.4 3.9 %collective-permute-start.10 = (bf16[64,2048]{1,0:T(8,128)(2,1)S(1)}, bf16[64,2048]{1,0:T(8,128)(2,1)S(1)}, u32[]{:S(2)}, u32[]{:S(2)}) collective-permute-start(bf16[64,2048]{1,0:T(8,128)(2,1)S(1)} %get-tuple-element.18), channel_id=1, source_target_pairs={{0,12},{2,14},{4,0},{6,2},{8,4},{10,6},{12,8},{14,10},{1,13},{3,15... | collective-permute-start | bytes 786440 | tf_op jit(solution)/shard_map/ppermute | solution.py:100
  212.4 14.2 %collective-permute-done.1 = bf16[4,64,2048]{2,1,0:T(8,128)(2,1)} collective-permute-done((bf16[4,64,2048]{2,1,0:T(8,128)(2,1)}, bf16[4,64,2048]{2,1,0:T(8,128)(2,1)}, u32[]{:S(2)}, u32[]{:S(2)}) %collective-permute-start.1) | collective-permute-done | bytes 1048608 | tf_op jit(solution)/shard_map/ppermute | solution.py:90
  228.3 1.8 collective-permute-start.2
  230.1 2.4 collective-permute-start.3
  234.2 5.3 %collective-permute-done.2 = bf16[64,2048]{1,0:T(8,128)(2,1)S(1)} collective-permute-done((bf16[64,2048]{1,0:T(8,128)(2,1)S(1)}, bf16[64,2048]{1,0:T(8,128)(2,1)S(1)}, u32[]{:S(2)}, u32[]{:S(2)}) %collective-permute-start.2) | collective-permute-done | bytes 262176 | tf_op jit(solution)/shard_map/ppermute | solution.py:100
  239.5 8.9 %collective-permute-done.3 = bf16[64,2048]{1,0:T(8,128)(2,1)S(1)} collective-permute-done((bf16[64,2048]{1,0:T(8,128)(2,1)S(1)}, bf16[64,2048]{1,0:T(8,128)(2,1)S(1)}, u32[]{:S(2)}, u32[]{:S(2)}) %collective-permute-start.3) | collective-permute-done | bytes 262176 | tf_op jit(solution)/shard_map/ppermute | solution.py:100
  (78 shorter events, 37.0 us)
Async XLA Ops:
  0.6 4.2 %copy-start = (bf16[128,2048]{1,0:T(8,128)(2,1)S(1)}, bf16[128,2048]{1,0:T(8,128)(2,1)}, u32[]{:S(2)}) copy-start(bf16[128,2048]{1,0:T(8,128)(2,1)} %param.10) | copy-start | bytes 1572868
  107.1 7.2 %copy-start.8 = (bf16[8,256,256]{2,1,0:T(8,128)(2,1)S(1)}, bf16[8,256,256]{2,1,0:T(8,128)(2,1)}, u32[]{:S(2)}) copy-start(bf16[8,256,256]{2,1,0:T(8,128)(2,1)} %get-tuple-element.8) | copy-start | bytes 3145732
  116.9 14.9 %collective-permute-start.14 = (bf16[128,2048]{1,0:T(8,128)(2,1)S(1)}, bf16[128,2048]{1,0:T(8,128)(2,1)S(1)}, u32[]{:S(2)}, u32[]{:S(2)}) collective-permute-start(bf16[128,2048]{1,0:T(8,128)(2,1)S(1)} %slice.94), channel_id=1, source_target_pairs={{0,16},{16,0},{1,17},{17,1},{2,18},{18,2},{3,19},{19,3},{4,20},{20... | collective-permute-start | bytes 1572872 | tf_op jit(solution)/shard_map/ppermute | solution.py:90
  122.7 23.7 %collective-permute-start.12 = (bf16[2048,128]{1,0:T(8,128)(2,1)}, bf16[2048,128]{1,0:T(8,128)(2,1)}, u32[]{:S(2)}, u32[]{:S(2)}) collective-permute-start(bf16[2048,128]{1,0:T(8,128)(2,1)} %slice.95), channel_id=1, source_target_pairs={{0,16},{16,0},{1,17},{17,1},{2,18},{18,2},{3,19},{19,3},{4,20},{20... | collective-permute-start | bytes 1572872 | tf_op jit(solution)/shard_map/ppermute | solution.py:90
  126.3 49.4 %collective-permute-start.6 = (bf16[2,4,64,2048]{3,2,1,0:T(8,128)(2,1)}, bf16[2,4,64,2048]{3,2,1,0:T(8,128)(2,1)}, u32[]{:S(2)}, u32[]{:S(2)}) collective-permute-start(bf16[2,4,64,2048]{3,2,1,0:T(8,128)(2,1)} %bitcast.19), channel_id=1, source_target_pairs={{0,1},{1,0},{2,3},{3,2},{4,5},{5,4},{6,7},{7,6},{8,9},{9,8},{10,11... | collective-permute-start | bytes 6291464 | tf_op jit(solution)/shard_map/ppermute | solution.py:90
  132.7 18.2 %all-to-all-start.1 = ((bf16[8,128,256]{2,1,0:T(8,128)(2,1)}), bf16[8,128,256]{2,1,0:T(8,128)(2,1)S(1)}, u32[]{:S(2)}, u32[]{:S(2)}) async-start(bf16[8,128,256]{2,1,0:T(8,128)(2,1)} %bitcast.83), calls=%async_computation.1 | async-start | bytes 1048576 | tf_op jit(solution)/shard_map/all_to_all | solution.py:373
  150.9 17.5 %all-to-all-start = ((bf16[8,256,128]{2,1,0:T(8,128)(2,1)}), bf16[8,256,128]{2,1,0:T(8,128)(2,1)S(1)}, u32[]{:S(2)}, u32[]{:S(2)}) async-start(bf16[8,256,128]{2,1,0:T(8,128)(2,1)} %bitcast.94), calls=%async_computation | async-start | bytes 1048576 | tf_op jit(solution)/shard_map/all_to_all | solution.py:371
  159.5 21.9 %collective-permute-start = (bf16[2,4,64,2048]{3,2,1,0:T(8,128)(2,1)}, bf16[2,4,64,2048]{3,2,1,0:T(8,128)(2,1)}, u32[]{:S(2)}, u32[]{:S(2)}) collective-permute-start(bf16[2,4,64,2048]{3,2,1,0:T(8,128)(2,1)} %bitcast.6), channel_id=1, source_target_pairs={{0,1},{1,0},{2,3},{3,2},{4,5},{5,4},{6,7},{7,6},{8,9},{9,8},{10,11... | collective-permute-start | bytes 6291464 | tf_op jit(solution)/shard_map/ppermute | solution.py:90
  159.5 14.9 %collective-permute-start.15 = (bf16[8,128,256]{2,1,0:T(8,128)(2,1)S(1)}, bf16[8,128,256]{2,1,0:T(8,128)(2,1)}, u32[]{:S(2)}, u32[]{:S(2)}) collective-permute-start(bf16[8,128,256]{2,1,0:T(8,128)(2,1)S(1)} %all-to-all-done.1), channel_id=1, source_target_pairs={{0,16},{16,0},{1,17},{17,1},{2,18},{18,2},{3,19},{19,3},{4,20},{20... | collective-permute-start | bytes 1572872 | tf_op jit(solution)/shard_map/ppermute | solution.py:90
  168.4 19.7 %collective-permute-start.13 = (bf16[8,256,128]{2,1,0:T(8,128)(2,1)S(1)}, bf16[8,256,128]{2,1,0:T(8,128)(2,1)S(1)}, u32[]{:S(2)}, u32[]{:S(2)}) collective-permute-start(bf16[8,256,128]{2,1,0:T(8,128)(2,1)S(1)} %all-to-all-done), channel_id=1, source_target_pairs={{0,16},{16,0},{1,17},{17,1},{2,18},{18,2},{3,19},{19,3},{4,20},{20... | collective-permute-start | bytes 1572872 | tf_op jit(solution)/shard_map/ppermute | solution.py:90
  178.1 5.6 %copy-start.2 = (bf16[2,4,64,2048]{3,2,1,0:T(8,128)(2,1)}, bf16[2,4,64,2048]{3,2,1,0:T(8,128)(2,1)S(1)}, u32[]{:S(2)}) copy-start(bf16[2,4,64,2048]{3,2,1,0:T(8,128)(2,1)S(1)} %fusion) | copy-start | bytes 6291460
  179.3 26.3 %collective-permute-start.7 = (bf16[4,64,2048]{2,1,0:T(8,128)(2,1)}, bf16[4,64,2048]{2,1,0:T(8,128)(2,1)}, u32[]{:S(2)}, u32[]{:S(2)}) collective-permute-start(bf16[4,64,2048]{2,1,0:T(8,128)(2,1)} %slice_bitcast_fusion), channel_id=1, source_target_pairs={{0,2},{2,0},{4,6},{6,4},{8,10},{10,8},{12,14},{14,12},{1,3},{3,1},... | collective-permute-start | bytes 3145736 | tf_op jit(solution)/shard_map/ppermute | solution.py:90
  184.8 41.8 %collective-permute-start.1 = (bf16[4,64,2048]{2,1,0:T(8,128)(2,1)}, bf16[4,64,2048]{2,1,0:T(8,128)(2,1)}, u32[]{:S(2)}, u32[]{:S(2)}) collective-permute-start(bf16[4,64,2048]{2,1,0:T(8,128)(2,1)} %slice_bitcast_fusion.2), channel_id=1, source_target_pairs={{0,2},{2,0},{4,6},{6,4},{8,10},{10,8},{12,14},{14,12},{1,3},{3,1},... | collective-permute-start | bytes 3145736 | tf_op jit(solution)/shard_map/ppermute | solution.py:90
  195.1 10.5 %copy-start.3 = (bf16[2,4,64,2048]{3,2,1,0:T(8,128)(2,1)S(1)}, bf16[2,4,64,2048]{3,2,1,0:T(8,128)(2,1)}, u32[]{:S(2)}) copy-start(bf16[2,4,64,2048]{3,2,1,0:T(8,128)(2,1)} %copy-done.2) | copy-start | bytes 6291460
  207.4 25.1 %collective-permute-start.10 = (bf16[64,2048]{1,0:T(8,128)(2,1)S(1)}, bf16[64,2048]{1,0:T(8,128)(2,1)S(1)}, u32[]{:S(2)}, u32[]{:S(2)}) collective-permute-start(bf16[64,2048]{1,0:T(8,128)(2,1)S(1)} %get-tuple-element.18), channel_id=1, source_target_pairs={{0,12},{2,14},{4,0},{6,2},{8,4},{10,6},{12,8},{14,10},{1,13},{3,15... | collective-permute-start | bytes 786440 | tf_op jit(solution)/shard_map/ppermute | solution.py:100
  211.2 22.7 %collective-permute-start.8 = (bf16[64,2048]{1,0:T(8,128)(2,1)S(1)}, bf16[64,2048]{1,0:T(8,128)(2,1)S(1)}, u32[]{:S(2)}, u32[]{:S(2)}) collective-permute-start(bf16[64,2048]{1,0:T(8,128)(2,1)S(1)} %get-tuple-element.17), channel_id=1, source_target_pairs={{0,4},{2,6},{4,8},{6,10},{8,12},{10,14},{12,0},{14,2},{1,5},{3,7},... | collective-permute-start | bytes 786440 | tf_op jit(solution)/shard_map/ppermute | solution.py:100
  211.3 22.7 %collective-permute-start.9 = (bf16[64,2048]{1,0:T(8,128)(2,1)S(1)}, bf16[64,2048]{1,0:T(8,128)(2,1)S(1)}, u32[]{:S(2)}, u32[]{:S(2)}) collective-permute-start(bf16[64,2048]{1,0:T(8,128)(2,1)S(1)} %get-tuple-element.19), channel_id=1, source_target_pairs={{0,8},{2,10},{4,12},{6,14},{8,0},{10,2},{12,4},{14,6},{1,9},{3,11}... | collective-permute-start | bytes 786440 | tf_op jit(solution)/shard_map/ppermute | solution.py:100
  228.3 20.4 %copy-start.5 = (bf16[128,2048]{1,0:T(8,128)(2,1)S(1)}, bf16[128,2048]{1,0:T(8,128)(2,1)}, u32[]{:S(2)}) copy-start(bf16[128,2048]{1,0:T(8,128)(2,1)} %param.9) | copy-start | bytes 1572868
  228.3 20.4 %copy-start.9 = (f32[2048]{0:T(1024)S(1)}, f32[2048]{0:T(1024)}, u32[]{:S(2)}) copy-start(f32[2048]{0:T(1024)} %param.11) | copy-start | bytes 24580
  228.3 11.1 %collective-permute-start.2 = (bf16[64,2048]{1,0:T(8,128)(2,1)S(1)}, bf16[64,2048]{1,0:T(8,128)(2,1)S(1)}, u32[]{:S(2)}, u32[]{:S(2)}) collective-permute-start(bf16[64,2048]{1,0:T(8,128)(2,1)S(1)} %get-tuple-element.20), channel_id=1, source_target_pairs={{0,4},{2,6},{4,8},{6,10},{8,12},{10,14},{12,0},{14,2},{1,5},{3,7},... | collective-permute-start | bytes 786440 | tf_op jit(solution)/shard_map/ppermute | solution.py:100
  230.1 18.2 %collective-permute-start.3 = (bf16[64,2048]{1,0:T(8,128)(2,1)S(1)}, bf16[64,2048]{1,0:T(8,128)(2,1)S(1)}, u32[]{:S(2)}, u32[]{:S(2)}) collective-permute-start(bf16[64,2048]{1,0:T(8,128)(2,1)S(1)} %get-tuple-element.22), channel_id=1, source_target_pairs={{0,8},{2,10},{4,12},{6,14},{8,0},{10,2},{12,4},{14,6},{1,9},{3,11}... | collective-permute-start | bytes 786440 | tf_op jit(solution)/shard_map/ppermute | solution.py:100
  232.5 15.9 %collective-permute-start.4 = (bf16[64,2048]{1,0:T(8,128)(2,1)S(1)}, bf16[64,2048]{1,0:T(8,128)(2,1)S(1)}, u32[]{:S(2)}, u32[]{:S(2)}) collective-permute-start(bf16[64,2048]{1,0:T(8,128)(2,1)S(1)} %get-tuple-element.21), channel_id=1, source_target_pairs={{0,12},{2,14},{4,0},{6,2},{8,4},{10,6},{12,8},{14,10},{1,13},{3,15... | collective-permute-start | bytes 786440 | tf_op jit(solution)/shard_map/ppermute | solution.py:100
  234.1 14.5 %collective-permute-start.11 = (bf16[64,2048]{1,0:T(8,128)(2,1)S(1)}, bf16[64,2048]{1,0:T(8,128)(2,1)S(1)}, u32[]{:S(2)}, u32[]{:S(2)}) collective-permute-start(bf16[64,2048]{1,0:T(8,128)(2,1)S(1)} %fusion.25), channel_id=1, source_target_pairs={{0,1},{1,0},{2,3},{3,2},{4,5},{5,4},{6,7},{7,6},{8,9},{9,8},{10,11... | collective-permute-start | bytes 786440 | tf_op jit(solution)/shard_map/ppermute | solution.py:90
  248.5 1.7 collective-permute-start.5
  (5 other events, 12.8 us)
where the time goes:
time: 255 us; the launch traced here: 251 us
  Pallas kernels  101 us (40%)
  waiting for transfers between devices  54.6 us (21%)
  starting transfers between devices  27.8 us (11%)
  local copies, waits for them, and re-layouts  25.5 us (10%)
  other arithmetic  25.4 us (10%)
  matrix products  15.6 us (6%)
    pallas_call x1, Pallas kernels, gather_all(): pl.pallas_call(functools.partial(gather_kernel, n_fs), out_shape=(jax.Sha...  101 us
    ppermute x10, waiting for transfers between devices, swap(): return lax.ppermute(values, axis, [(i, i ^ 1) for i in range(size)])  30.8 us
    ppermute x6, waiting for transfers between devices, line_shift(): lax.ppermute(values, 'fs', [(i, (i // 2 + shift) % outer * 2 + i % 2) for...  14.2 us
    ppermute x6, starting transfers between devices, line_shift(): lax.ppermute(values, 'fs', [(i, (i // 2 + shift) % outer * 2 + i % 2) for...  10.6 us
    dot_general x1, matrix products, hidden_body(): jnp.dot(hidden_later, down_own, preferred_element_type=jnp.float32)  9.08 us
    ppermute x10, starting transfers between devices, swap(): return lax.ppermute(values, axis, [(i, i ^ 1) for i in range(size)])  8.8 us
    convert_element_type x4, other arithmetic, scatter_tokens(): (blocks[0].astype(jnp.float32) + got.astype(jnp.float32)).astype(jnp.bflo...  7.97 us
    all_to_all x1, waiting for transfers between devices, hidden_body(): lax.all_to_all(up_half.reshape(n_fs, depth, part), 'fs', 0, 0, tiled=True)  7.39 us
  transfers between devices with their start and end apart: 18, of which 8 were waited for; matrix products, arithmetic and copies ran while one was open for 20% of the time, Pallas kernels for 0%

commit v1 on v0

v1 whole, which is shorter than its diff:
```python
import functools

import jax
import jax.numpy as jnp
from jax import lax
from jax.experimental import pallas as pl
from jax.experimental.pallas import tpu as pltpu
from jax.sharding import PartitionSpec as P

EPSILON = 1e-06
MESH = pl.DeviceIdType.MESH
TRANSPOSED = (((1,), (1,)), ((), ()))
LEADING = (((0,), (0,)), ((), ()))
X, Y, Z = 4, 2, 1
COT, SAVED, LATER = 0, 1, 2
BACK, MIXED = 0, 1
UP, DOWN = 0, 1
VMEM_BYTES = 64 * 2**20 - 2**16


def norm_partial_terms(values, norm_gain_vector):
    floats = values.astype(jnp.float32)
    inverse = lax.rsqrt(jnp.mean(floats * floats, axis=-1, keepdims=True) + EPSILON)
    unit_rows = floats * inverse
    normed = (unit_rows * norm_gain_vector).astype(jnp.bfloat16)
    return (inverse, unit_rows, normed)


def squared_relu(pre_act):
    return jnp.square(jax.nn.relu(pre_act)).astype(jnp.bfloat16)


def body(
    x_later, kept_input_rows, cotangent, norm_gain_vector, up_weight, down_weight, up_sum, down_sum
):
    row_count = x_later.shape[0]
    grad_scale = float(row_count * lax.axis_size("rep") * lax.axis_size("fs")) ** (-0.5)
    inv_later, unit_later, normed_later = norm_partial_terms(x_later, norm_gain_vector)
    inverse_rms_kept, unit_kept_rows, normed_kept_rows = norm_partial_terms(
        kept_input_rows, norm_gain_vector
    )
    stacked = jnp.concatenate([normed_kept_rows, normed_later], axis=0)
    up_whole = lax.all_gather(up_weight, "fs", axis=0, tiled=True)
    down_whole = lax.all_gather(down_weight, "fs", axis=1, tiled=True)
    pre_act = jnp.dot(stacked, up_whole, preferred_element_type=jnp.float32)
    pre_saved = pre_act[:row_count]
    hidden_saved = squared_relu(pre_saved)
    hidden_later = squared_relu(pre_act[row_count:])
    mixed_part = jnp.dot(hidden_later, down_whole, preferred_element_type=jnp.float32)
    hidden_grad = lax.dot_general(
        cotangent, down_whole, TRANSPOSED, preferred_element_type=jnp.float32
    )
    pre_grad = (hidden_grad * 2.0 * jax.nn.relu(pre_saved)).astype(jnp.bfloat16)
    back_part = lax.dot_general(pre_grad, up_whole, TRANSPOSED, preferred_element_type=jnp.float32)
    mixed_sum, back_sum = (
        lax.psum(mixed_part.astype(jnp.bfloat16), "tp").astype(jnp.float32),
        lax.psum(back_part.astype(jnp.bfloat16), "tp").astype(jnp.float32),
    )
    mixed = mixed_sum.astype(jnp.bfloat16)
    scaled_rows = back_sum * norm_gain_vector
    input_gradient_rows = (
        inverse_rms_kept
        * (
            scaled_rows
            - unit_kept_rows * jnp.mean(scaled_rows * unit_kept_rows, axis=-1, keepdims=True)
        )
    ).astype(jnp.bfloat16)
    cot_columns, normed_columns = (
        lax.all_to_all(cotangent, "fs", split_axis=1, concat_axis=0, tiled=True),
        lax.all_to_all(normed_kept_rows, "fs", split_axis=1, concat_axis=0, tiled=True),
    )
    columns = normed_columns
    up_grad = grad_scale * lax.dot_general(
        columns,
        lax.all_gather(pre_grad, "fs", axis=0, tiled=True),
        LEADING,
        preferred_element_type=jnp.float32,
    )
    columns = cot_columns
    down_grad = lax.dot_general(
        lax.all_gather(hidden_saved, "fs", axis=0, tiled=True),
        columns,
        LEADING,
        preferred_element_type=jnp.float32,
    )
    up_added, down_added = (
        lax.psum(up_grad.astype(jnp.bfloat16), "rep").astype(jnp.float32),
        lax.psum((down_grad * grad_scale).astype(jnp.bfloat16), "rep").astype(jnp.float32),
    )
    return (mixed, input_gradient_rows, up_sum + up_added, down_sum + down_added)

def layer_kernel(
    n_fs, grad_scale, x_ref, kept_ref, cot_ref, gain_ref, up_ref, down_ref,
    mixed_out, input_out, up_out, down_out,
    tok, up_own, down_own, up_pass, down_pass, hidden, pre_grad,
    grad_kept, grad_sent, grad_got, grad_sum, grad_line, grad_pair, grad_all,
    part, got_first, got_second, got_third, rows_out,
    pair_send, pair_recv, line_send, line_recv, core_send, core_recv, own_sem,
    tok_send, tok_recv, share_send, share_recv, gline_send, gline_recv,
    gpair_send, gpair_recv, grep_send, grep_recv, part_send, part_recv, out_send, out_recv,
):
    rep, fs, core = lax.axis_index("rep"), lax.axis_index("fs"), lax.axis_index("tp")
    outer = n_fs // 2
    place, pair = fs // 2, fs % 2
    low = place % 2
    rows, width = tok.shape[2:]
    depth, own = up_pass.shape
    n_slots = tok.shape[1]
    tokens = n_slots * rows
    other_core = (rep, fs, 1 - core)
    start_row = pl.multiple_of(core * rows, rows)

    def place_at(step):
        return (place, place + 1 - 2 * low, (place + 2) % outer, outer - 1 - place)[step]

    def line_peer(step):
        return (rep, place_at(step) * 2 + pair, core)

    def partner(dim):
        if dim == X:
            return (1 - rep, fs, core)
        if dim == Y:
            return (rep, place * 2 + 1 - pair, core)
        return line_peer(1)

    def flip(bit, on):
        return 1 - bit if on else bit

    def slot(mask):
        return flip(rep, mask & X) * 4 + flip(pair, mask & Y) * 2 + flip(low, mask & Z)

    def block(rep_at, pair_at, low_at):
        return (rep_at * 2 + pair_at) * 2 + low_at

    def copy(source, target, send, recv, device):
        return pltpu.make_async_remote_copy(
            src_ref=source, dst_ref=target, send_sem=send, recv_sem=recv,
            device_id=device, device_id_type=MESH,
        )

    sent = []

    def go(source, target, send, recv, device):
        one = copy(source, target, send, recv, device)
        one.start()
        sent.append(one)

    def landed(target, sem):
        copy(target, target, sem, sem, other_core).wait_recv()

    barrier = pltpu.get_barrier_semaphore()
    peers = [other_core, partner(X), partner(Y)] + [line_peer(step) for step in range(1, outer)]
    for peer in peers:
        pl.semaphore_signal(barrier, inc=1, device_id=peer, device_id_type=MESH)

    gain = gain_ref[...]
    own_rows = pl.ds(start_row, rows)
    tok[COT, slot(0)] = cot_ref[own_rows, :]
    tok[SAVED, slot(0)] = norm_partial_terms(kept_ref[own_rows, :], gain)[2]
    tok[LATER, slot(0)] = norm_partial_terms(x_ref[own_rows, :], gain)[2]
    pl.semaphore_wait(barrier, len(peers))

    def up_source(index):
        return up_ref.at[:, pl.ds(pl.multiple_of(index * own, own), own)]

    def down_source(index):
        return down_ref.at[pl.ds(pl.multiple_of(index * own, own), own), :]

    def up_slot(half, place_to, pair_to, count=1):
        first = pl.multiple_of((place_to * 2 + pair_to) * depth, depth)
        return up_own.at[half, pl.ds(first, count * depth), :]

    def down_slot(half, place_to, pair_to, count=1):
        first = pl.multiple_of((place_to * 2 + pair_to) * depth, depth)
        return down_own.at[half, :, pl.ds(first, count * depth)]

    def send_tok(array, mask, dim):
        at = tok.at[array, slot(mask)]
        key = token_sends.setdefault((array, mask, dim), len([k for k in token_sends if k[0] == array]))
        go(at, at, tok_send.at[array, key], tok_recv.at[array, (mask ^ dim) - 1], partner(dim))

    token_sends = {}

    def tok_landed(array, mask):
        landed(tok.at[array, slot(mask)], tok_recv.at[array, mask - 1])

    orders = {COT: (Y, X), SAVED: (Y, X), LATER: (X, Y)}

    def tok_begin(array):
        for dim in (Z,) + orders[array]:
            send_tok(array, 0, dim)

    def tok_step(array, stage):
        second, third = orders[array]
        mask = (Z, second, second | Z)[stage]
        tok_landed(array, mask)
        if stage == 0:
            send_tok(array, mask, second)
        send_tok(array, mask, third)

    def tok_end(array):
        third = orders[array][1]
        for mask in (0, Z, orders[array][0], orders[array][0] | Z):
            tok_landed(array, third | mask)

    for which, low_to in enumerate((low, 1 - low)):
        index = block(rep, 1 - pair, low_to)
        up_to = up_pass if which else up_slot(core, place, pair)
        down_to = down_pass if which else down_slot(core, place, pair)
        go(up_source(index), up_to, pair_send.at[which, UP], pair_recv.at[which, UP], partner(Y))
        go(down_source(index), down_to, pair_send.at[which, DOWN], pair_recv.at[which, DOWN], partner(Y))
    for array in (COT, SAVED):
        tok_begin(array)
    keep = [
        pltpu.make_async_copy(up_source(block(rep, pair, low)), up_slot(core, place, pair), own_sem.at[UP]),
        pltpu.make_async_copy(down_source(block(rep, pair, low)), down_slot(core, place, pair), own_sem.at[DOWN]),
    ]
    for one in keep:
        one.start()
    steps = (3, 2, 1)
    for step in steps:
        index = block(rep, pair, flip(low, step % 2))
        sems = (line_send.at[step - 1, 0], line_recv.at[step - 1, 0])
        go(up_source(index), up_slot(core, place, pair), sems[0].at[UP], sems[1].at[UP], line_peer(step))
        go(down_source(index), down_slot(core, place, pair), sems[0].at[DOWN], sems[1].at[DOWN], line_peer(step))

    def to_core(step):
        at = place_at(step)
        go(
            up_slot(core, at, 0, 2), up_slot(core, at, 0, 2),
            core_send.at[step, UP], core_recv.at[step, UP], other_core,
        )
        go(
            down_slot(core, at, 0, 2), down_slot(core, at, 0, 2),
            core_send.at[step, DOWN], core_recv.at[step, DOWN], other_core,
        )

    tok_step(COT, 0)
    for which in range(2):
        landed(up_pass if which else up_slot(core, place, 1 - pair), pair_recv.at[which, UP])
        landed(down_pass if which else down_slot(core, place, 1 - pair), pair_recv.at[which, DOWN])
    for step in steps:
        up_from = up_pass if step % 2 else up_slot(core, place, 1 - pair)
        down_from = down_pass if step % 2 else down_slot(core, place, 1 - pair)
        sems = (line_send.at[step - 1, 1], line_recv.at[step - 1, 1])
        go(up_from, up_slot(core, place, 1 - pair), sems[0].at[UP], sems[1].at[UP], line_peer(step))
        go(down_from, down_slot(core, place, 1 - pair), sems[0].at[DOWN], sems[1].at[DOWN], line_peer(step))
    tok_step(SAVED, 0)
    for one in keep:
        one.wait()
    to_core(0)
    for stage in (1, 2):
        tok_step(COT, stage)
        tok_step(SAVED, stage)
    tok_begin(LATER)
    for step in (1, 2, 3):
        at = place_at(step)
        for part_of, pair_at in enumerate((pair, 1 - pair)):
            landed(up_slot(core, at, pair_at), line_recv.at[step - 1, part_of, UP])
            landed(down_slot(core, at, pair_at), line_recv.at[step - 1, part_of, DOWN])
        to_core(step)
    tok_end(COT)
    tok_end(SAVED)
    for step in range(outer):
        at = place_at(step)
        landed(up_slot(1 - core, at, 0, 2), core_recv.at[step, UP])
        landed(down_slot(1 - core, at, 0, 2), core_recv.at[step, DOWN])

    def all_tokens(array):
        return tok[array].reshape(tokens, width)

    @pl.loop(0, 2)
    def _(half):
        pre = jnp.dot(all_tokens(SAVED), up_own[half], preferred_element_type=jnp.float32)
        grad = lax.dot_general(
            all_tokens(COT), down_own[half], TRANSPOSED, preferred_element_type=jnp.float32
        )
        hidden[half] = squared_relu(pre)
        pre_grad[half] = (grad * 2.0 * jax.nn.relu(pre)).astype(jnp.bfloat16)

    tok_step(LATER, 0)

    chunk = width // outer

    def chunk_at(index):
        return pl.ds(pl.multiple_of(index * chunk, chunk), chunk)

    def weight_grad(kind, half, columns):
        left = hidden[half] if kind == DOWN else pre_grad[half]
        right = tok[COT if kind == DOWN else SAVED, :, :, columns].reshape(tokens, chunk)
        return grad_scale * lax.dot_general(left, right, LEADING, preferred_element_type=jnp.float32)

    for kind in (UP, DOWN):

        @pl.loop(0, outer)
        def _(index):
            columns = chunk_at(index)
            grad_sent[kind, :, columns] = weight_grad(kind, 1 - core, columns).astype(jnp.bfloat16)

        go(grad_sent.at[kind], grad_got.at[kind], share_send.at[kind], share_recv.at[kind], other_core)

    tok_step(LATER, 1)
    for kind in (UP, DOWN):

        @pl.loop(0, outer)
        def _(index):
            columns = chunk_at(index)
            grad_kept[kind, :, columns] = weight_grad(kind, core, columns)

    for kind in (UP, DOWN):
        landed(grad_got.at[kind], share_recv.at[kind])

        @pl.loop(0, outer)
        def _(index):
            columns = chunk_at(index)
            grad_sum[kind, :, columns] = (
                grad_kept[kind, :, columns] + grad_got[kind, :, columns].astype(jnp.float32)
            ).astype(jnp.bfloat16)

        for step in steps:
            go(
                grad_sum.at[kind, :, chunk_at(place_at(step))], grad_line.at[step - 1, kind],
                gline_send.at[step - 1, kind], gline_recv.at[step - 1, kind], line_peer(step),
            )

    @pl.loop(0, outer)
    def _(index):
        columns = chunk_at(index)
        total = jnp.zeros((tokens, chunk), jnp.float32)
        for half in range(2):
            total = total + lax.dot_general(
                pre_grad[half], up_own[half, columns, :], TRANSPOSED, preferred_element_type=jnp.float32
            )
        part[BACK, :, :, columns] = total.astype(jnp.bfloat16).reshape(n_slots, rows, chunk)

    sum_orders = {BACK: (X, Y), MIXED: (Y, X)}

    def part_first(array):
        first, second = sum_orders[array]
        for number, mask in enumerate((second | Z, second, Z, 0)):
            go(
                part.at[array, slot(first | mask)], got_first.at[array, number],
                part_send.at[array, number], part_recv.at[array, number], partner(first),
            )

    def part_add(array, mask, *got):
        total = part[array, slot(mask)].astype(jnp.float32)
        for one in got:
            total = total + one[...].astype(jnp.float32)
        return total

    def part_second(array):
        first, second = sum_orders[array]
        for number, mask in enumerate((second | Z, second)):
            landed(got_first.at[array, number], part_recv.at[array, number])
            part[array, slot(mask)] = part_add(array, mask, got_first.at[array, number]).astype(jnp.bfloat16)
            go(
                part.at[array, slot(mask)], got_second.at[array, number],
                part_send.at[array, 4 + number], part_recv.at[array, 4 + number], partner(second),
            )

    def part_third(array):
        landed(got_first.at[array, 2], part_recv.at[array, 2])
        landed(got_second.at[array, 0], part_recv.at[array, 4])
        part[array, slot(Z)] = part_add(
            array, Z, got_first.at[array, 2], got_second.at[array, 0]
        ).astype(jnp.bfloat16)
        go(
            part.at[array, slot(Z)], got_third.at[array],
            part_send.at[array, 6], part_recv.at[array, 6], partner(Z),
        )

    def part_last(array):
        landed(got_first.at[array, 3], part_recv.at[array, 3])
        landed(got_second.at[array, 1], part_recv.at[array, 5])
        landed(got_third.at[array], part_recv.at[array, 6])
        return part_add(array, 0, got_first.at[array, 3], got_second.at[array, 1], got_third.at[array])

    part_first(BACK)

    tok_step(LATER, 2)
    tok_end(LATER)

    @pl.loop(0, 2)
    def _(half):
        hidden[half] = squared_relu(
            jnp.dot(all_tokens(LATER), up_own[half], preferred_element_type=jnp.float32)
        )

    @pl.loop(0, outer)
    def _(index):
        columns = chunk_at(index)
        total = jnp.zeros((tokens, chunk), jnp.float32)
        for half in range(2):
            total = total + jnp.dot(
                hidden[half], down_own[half, :, columns], preferred_element_type=jnp.float32
            )
        part[MIXED, :, :, columns] = total.astype(jnp.bfloat16).reshape(n_slots, rows, chunk)

    part_first(MIXED)
    part_second(BACK)

    def line_part(kind, which, pair_at):
        inside = pl.ds(pl.multiple_of(pair_at * depth, depth), depth)
        if which:
            total = grad_line[0, kind, :, inside].astype(jnp.float32)
            total = total + grad_line[2, kind, :, inside].astype(jnp.float32)
        else:
            mine = pl.ds(pl.multiple_of((place * 2 + pair_at) * depth, depth), depth)
            total = grad_sum[kind, :, mine].astype(jnp.float32)
            total = total + grad_line[1, kind, :, inside].astype(jnp.float32)
        return (total.T if kind == UP else total).astype(jnp.bfloat16)

    def blocks_at(kind, rep_at, pair_at):
        return grad_all.at[kind, pl.ds(block(rep_at, pair_at, 0), 2)]

    def grad_spread(kind):
        for step in steps:
            landed(grad_line.at[step - 1, kind], gline_recv.at[step - 1, kind])
        for which, low_at in enumerate((low, 1 - low)):
            grad_pair[kind, low_at] = line_part(kind, which, 1 - pair)
        go(
            grad_pair.at[kind], blocks_at(kind, rep, pair),
            gpair_send.at[kind], gpair_recv.at[kind], partner(Y),
        )
        for which, low_at in enumerate((low, 1 - low)):
            grad_all[kind, block(rep, pair, low_at)] = line_part(kind, which, pair)
        mine = blocks_at(kind, rep, pair)
        go(mine, mine, grep_send.at[kind, 0], grep_recv.at[kind, 0], partner(X))

    def grad_pass(kind):
        near = blocks_at(kind, rep, 1 - pair)
        landed(near, gpair_recv.at[kind])
        go(near, near, grep_send.at[kind, 1], grep_recv.at[kind, 1], partner(X))

    part_third(BACK)
    grad_spread(UP)
    part_second(MIXED)
    grad_pass(UP)

    back_sum = part_last(BACK)
    inverse, unit_rows, _ = norm_partial_terms(kept_ref[own_rows, :], gain)
    scaled_rows = back_sum * gain
    rows_out[BACK, core] = (
        inverse * (scaled_rows - unit_rows * jnp.mean(scaled_rows * unit_rows, axis=-1, keepdims=True))
    ).astype(jnp.bfloat16)

    def share_rows(array):
        mine = rows_out.at[array, core]
        go(mine, mine, out_send.at[array], out_recv.at[array], other_core)

    share_rows(BACK)
    part_third(MIXED)
    grad_spread(DOWN)
    rows_out[MIXED, core] = part_last(MIXED).astype(jnp.bfloat16)
    share_rows(MIXED)
    grad_pass(DOWN)

    for array, out in ((BACK, input_out), (MIXED, mixed_out)):
        landed(rows_out.at[array, 1 - core], out_recv.at[array])
        out[...] = rows_out[array].reshape(2 * rows, width)
    for kind in (UP, DOWN):
        for number, pair_at in enumerate((pair, 1 - pair)):
            landed(blocks_at(kind, 1 - rep, pair_at), grep_recv.at[kind, number])
        for index in range(n_fs):
            if kind == UP:
                up_out[:, index * own : (index + 1) * own] = grad_all[UP, index]
            else:
                down_out[index * own : (index + 1) * own, :] = grad_all[DOWN, index]
    for one in sent:
        one.wait_send()


def cube_body(
    x_later, kept_input_rows, cotangent, norm_gain_vector, up_weight, down_weight, up_sum, down_sum
):
    row_count, width = x_later.shape
    n_fs = lax.axis_size("fs")
    grad_scale = float(row_count * lax.axis_size("rep") * n_fs) ** (-0.5)
    depth, units = up_weight.shape
    own = units // n_fs
    rows = row_count // 2
    outer = n_fs // 2
    tokens = n_fs * rows
    kind = x_later.dtype
    dma = pltpu.SemaphoreType.DMA
    vmem = functools.partial(pltpu.VMEM, dtype=kind)
    inside = pl.BlockSpec(memory_space=pltpu.VMEM)
    outside = pl.BlockSpec(memory_space=pl.ANY)
    mixed, input_gradient_rows, up_added, down_added = pl.pallas_call(
        functools.partial(layer_kernel, n_fs, grad_scale),
        out_shape=(
            jax.ShapeDtypeStruct((row_count, width), kind),
            jax.ShapeDtypeStruct((row_count, width), kind),
            jax.ShapeDtypeStruct((depth, units), kind),
            jax.ShapeDtypeStruct((units, depth), kind),
        ),
        in_specs=[inside] * 4 + [outside] * 2,
        out_specs=[inside] * 4,
        scratch_shapes=[
            vmem((3, n_fs, rows, width)),
            vmem((2, width, own)), vmem((2, own, width)), vmem((depth, own)), vmem((own, depth)),
            vmem((2, tokens, own)), vmem((2, tokens, own)),
            pltpu.VMEM((2, own, width), jnp.float32),
            vmem((2, own, width)), vmem((2, own, width)), vmem((2, own, width)),
            vmem((3, 2, own, 2 * depth)), vmem((2, 2, own, depth)), vmem((2, n_fs, own, depth)),
            vmem((2, n_fs, rows, width)),
            vmem((2, 4, rows, width)), vmem((2, 2, rows, width)), vmem((2, rows, width)),
            vmem((2, 2, rows, width)),
            dma((2, 2)), dma((2, 2)), dma((3, 2, 2)), dma((3, 2, 2)), dma((outer, 2)), dma((outer, 2)),
            dma((2,)), dma((3, 7)), dma((3, 7)), dma((2,)), dma((2,)), dma((3, 2)), dma((3, 2)),
            dma((2,)), dma((2,)), dma((2, 2)), dma((2, 2)), dma((2, 7)), dma((2, 7)), dma((2,)), dma((2,)),
        ],
        compiler_params=pltpu.CompilerParams(
            collective_id=0, has_side_effects=True, vmem_limit_bytes=VMEM_BYTES
        ),
    )(
        x_later, kept_input_rows, cotangent, norm_gain_vector.reshape(1, width), up_weight, down_weight,
    )
    return (
        mixed,
        input_gradient_rows,
        up_sum + up_added.astype(jnp.float32),
        down_sum + down_added.astype(jnp.float32),
    )


def chosen_body(*args):
    depth, units = args[4].shape
    n_fs = lax.axis_size("fs")
    cubes = lax.axis_size("tp") == 2 and lax.axis_size("rep") == 2 and n_fs == 8
    return (cube_body if cubes and units == depth * n_fs and depth % 128 == 0 else body)(*args)


def solution(mesh):
    return jax.shard_map(
        chosen_body,
        mesh=mesh,
        in_specs=(
            P(("rep", "fs"), None),
            P(("rep", "fs"), None),
            P(("rep", "fs"), None),
            P(),
            P("fs", "tp"),
            P("tp", "fs"),
            P("fs", "tp"),
            P("tp", "fs"),
        ),
        out_specs=(P(("rep", "fs"), None), P(("rep", "fs"), None), P("fs", "tp"), P("tp", "fs")),
        check_vma=False,
    )
```

time: 255 us -> 157 us (0.62); the launches traced: 251 us -> 157 us
  waiting for transfers between devices: 54.6 us -> 0 us
  Pallas kernels: 101 us -> 149 us
  starting transfers between devices: 27.8 us -> 0 us
  local copies, waits for them, and re-layouts: 25.5 us -> 1.6 us
  other arithmetic: 25.4 us -> 5.22 us
  matrix products: 15.6 us -> 0 us
    pallas_call x1, Pallas kernels: 101 us -> 149 us  [cube_body(): pl.pallas_call(functools.partial(layer_kernel, n_fs, grad_scale), out_sha...]
    ppermute x16 -> x0, waiting for transfers between devices: 45 us -> none  [the longest x10 30.8 us: swap(): return lax.ppermute(values, axis, [(i, i ^ 1) for i in range(size)])]
    ppermute x16 -> x0, starting transfers between devices: 19.4 us -> none  [the longest x6 10.6 us: line_shift(): lax.ppermute(values, 'fs', [(i, (i // 2 + shift) % outer * 2 + i % 2) for...]
    dot_general x6 -> x0, matrix products: 15.6 us -> none  [the longest x1 9.08 us: hidden_body(): jnp.dot(hidden_later, down_own, preferred_element_type=jnp.float32)]
    convert_element_type x12 -> x0, other arithmetic: 14.9 us -> none  [the longest x4 7.97 us: scatter_tokens(): (blocks[0].astype(jnp.float32) + got.astype(jnp.float32)).astype(jnp.bflo...]
    slice x5 -> x0, local copies, waits for them, and re-layouts: 14.8 us -> none  [the longest x1 7.2 us: hidden_body(): tok[i].reshape(-1, width)]
    all_to_all x2 -> x0, waiting for transfers between devices: 9.63 us -> none  [the longest x1 7.39 us: hidden_body(): lax.all_to_all(up_half.reshape(n_fs, depth, part), 'fs', 0, 0, tiled=True)]
    all_to_all x2 -> x0, starting transfers between devices: 8.35 us -> none  [the longest x1 4.59 us: hidden_body(): down_half = lax.all_to_all(down_half, 'fs', 0, 0, tiled=True)]
  transfers between devices with their start and end apart: 18 -> 0, of which waited for: 8 -> 0; matrix products, arithmetic and copies ran while one was open for 20% -> 0% of each run, Pallas kernels for 0% -> 0%
where the time goes in v1:
time: 157 us
  Pallas kernels  149 us (95%)
  other arithmetic  5.22 us (3%)
  local copies, waits for them, and re-layouts  1.6 us (1%)
    pallas_call x1, Pallas kernels, cube_body(): pl.pallas_call(functools.partial(layer_kernel, n_fs, grad_scale), out_sha...  149 us
    add x1, other arithmetic, cube_body(): up_sum + up_added.astype(jnp.float32)  3.7 us

profile of v1, /device:TPU:0, one launch (start us, length us, event | category | flops | bytes accessed | tf_op | source)
XLA Modules:
  0.0 156.5 jit_solution(9585707857804342188)
XLA Ops:
  0.6 149.0 %shard_map.111 = (bf16[128,2048]{1,0:T(8,128)(2,1)}, bf16[128,2048]{1,0:T(8,128)(2,1)}, bf16[256,2048]{1,0:T(8,128)(2,1)}, bf16[2048,256]{1,0:T(8,128)(2,1)}) custom-call(bf16[128,2048]{1,0:T(8,128)(2,1)} %x_ref.1, bf16[128,2048]{1,0:T(8,128)(2,1)} %kept_ref.1, bf16[128,2048]{1,0:T(8,128)(2,1)} %cot_ref.1, f32[1,2048]{1,0:T(1,128)} %bitcast.1, ...), custom_call_target="tpu_custom_call" | custom-call | tf_op jit(solution)/shard_map/pallas_call | solution.py:490
  149.6 0.0 copy-start
  149.7 0.0 copy-start.1
  149.7 3.7 %convert_add_fusion.1 = f32[256,2048]{1,0:T(8,128)} fusion(f32[256,2048]{1,0:T(8,128)} %param.14, bf16[256,2048]{1,0:T(8,128)(2,1)} %get-tuple-element.10), kind=kLoop, calls=%fused_computation.1 | loop fusion | flops 1048576 | bytes 5242880 | tf_op jit(solution)/shard_map/add | solution.py:523
  153.4 0.0 copy-done
  153.4 0.0 copy-done.1
  153.4 0.0 copy-start.3
  153.4 0.0 copy-start.2
  153.4 1.5 convert_add_fusion
  154.9 0.0 copy-done.3
  154.9 0.8 copy.14
  155.7 0.0 copy-done.2
  155.7 0.8 copy.15
Async XLA Ops:
  149.6 3.7 %copy-start = (f32[2048,256]{1,0:T(8,128)S(1)}, f32[2048,256]{1,0:T(8,128)}, u32[]{:S(2)}) copy-start(f32[2048,256]{1,0:T(8,128)} %param.15) | copy-start | bytes 6291460
  149.7 3.7 %copy-start.1 = (bf16[2048,256]{1,0:T(8,128)(2,1)S(1)}, bf16[2048,256]{1,0:T(8,128)(2,1)}, u32[]{:S(2)}) copy-start(bf16[2048,256]{1,0:T(8,128)(2,1)} %get-tuple-element.11) | copy-start | bytes 3145732
  153.4 1.5 copy-start.3
  153.4 2.3 %copy-start.2 = (bf16[128,2048]{1,0:T(8,128)(2,1)S(1)}, bf16[128,2048]{1,0:T(8,128)(2,1)}, u32[]{:S(2)}) copy-start(bf16[128,2048]{1,0:T(8,128)(2,1)} %get-tuple-element.17) | copy-start | bytes 1572868

commit v2 on v1

v2 whole, which is shorter than its diff:
```python
import functools

import jax
import jax.numpy as jnp
from jax import lax
from jax.experimental import pallas as pl
from jax.experimental.pallas import tpu as pltpu
from jax.sharding import PartitionSpec as P

EPSILON = 1e-06
MESH = pl.DeviceIdType.MESH
TRANSPOSED = (((1,), (1,)), ((), ()))
LEADING = (((0,), (0,)), ((), ()))
X, Y, Z = 4, 2, 1
COT, SAVED, LATER = 0, 1, 2
BACK, MIXED = 0, 1
UP, DOWN = 0, 1
(TOK, PAIR, LINE, LINE_PASS, CORE, PRE, GRAD, SHARE, KEEP, GRAD_LINE,
 GRAD_PAIR, GRAD_REP, BACK_SUMS, MIXED_SUMS, FIRST, SECOND, THIRD, LAST, END, TOKENS, OWN, PARTS, ROWS) = range(23)
KIND_ORDER = (DOWN, UP)
SUM_ORDERS = (((X, Y), (Y, X)), ((X, Y), (Y, X)))
SCHEDULE = (
    (TOK, COT, 0, Y), (PAIR, UP), (TOK, COT, 0, X), (TOK, SAVED, 0, Y), (TOK, LATER, 0, X),
    (TOK, SAVED, 0, Z), (LINE, UP), (TOK, SAVED, 0, X), (TOK, COT, Y, X), (TOK, COT, 0, Z),
    (TOK, SAVED, Z, Y), (PAIR, DOWN), (LINE_PASS, UP), (TOK, SAVED, Z, X), (TOK, SAVED, Y, X),
    (TOK, LATER, 0, Y), (TOK, COT, Z, Y), (CORE, UP, 0), (TOK, LATER, 0, Z), (LINE_PASS, DOWN),
    (TOK, COT, Z, X), (TOK, LATER, X, Y), (LINE, DOWN), (CORE, UP, 2), (CORE, UP, 3),
    (CORE, DOWN, 0), (CORE, UP, 1), (TOK, SAVED, Y | Z, X), (TOK, COT, Y | Z, X),
    (TOK, LATER, Z, X), (PRE, 1), (TOK, LATER, Z, Y), (PRE, 0), (CORE, DOWN, 1), (KEEP, DOWN),
    (SHARE, DOWN), (CORE, DOWN, 3), (CORE, DOWN, 2), (GRAD_LINE, DOWN), (GRAD, 0), (GRAD, 1),
    (BACK_SUMS,), (FIRST, BACK, 0, 0), (TOK, LATER, X | Z, Y), (FIRST, BACK, 0, 1),
    (FIRST, BACK, 1, 0), (MIXED_SUMS,), (SECOND, BACK, 1, 0), (KEEP, UP), (FIRST, MIXED, 0, 0),
    (SECOND, BACK, 0, 1), (FIRST, MIXED, 0, 1), (SHARE, UP), (GRAD_PAIR, DOWN, 0),
    (FIRST, MIXED, 1, 1), (SECOND, BACK, 0, 0), (SECOND, MIXED, 0, 0), (GRAD_LINE, UP),
    (FIRST, MIXED, 1, 0), (FIRST, BACK, 1, 1), (GRAD_REP, DOWN), (GRAD_PAIR, DOWN, 1),
    (THIRD, BACK, 0), (THIRD, MIXED, 0), (SECOND, BACK, 1, 1), (SECOND, MIXED, 1, 0),
    (SECOND, MIXED, 1, 1), (GRAD_PAIR, UP, 0), (GRAD_PAIR, UP, 1), (THIRD, BACK, 1), (GRAD_REP, UP),
    (THIRD, MIXED, 1), (SECOND, MIXED, 0, 1), (LAST, BACK), (LAST, MIXED), (END,),
)
VMEM_BYTES = 64 * 2**20 - 2**16


def norm_partial_terms(values, norm_gain_vector):
    floats = values.astype(jnp.float32)
    inverse = lax.rsqrt(jnp.mean(floats * floats, axis=-1, keepdims=True) + EPSILON)
    unit_rows = floats * inverse
    normed = (unit_rows * norm_gain_vector).astype(jnp.bfloat16)
    return (inverse, unit_rows, normed)


def squared_relu(pre_act):
    return jnp.square(jax.nn.relu(pre_act)).astype(jnp.bfloat16)


def body(
    x_later, kept_input_rows, cotangent, norm_gain_vector, up_weight, down_weight, up_sum, down_sum
):
    row_count = x_later.shape[0]
    grad_scale = float(row_count * lax.axis_size("rep") * lax.axis_size("fs")) ** (-0.5)
    inv_later, unit_later, normed_later = norm_partial_terms(x_later, norm_gain_vector)
    inverse_rms_kept, unit_kept_rows, normed_kept_rows = norm_partial_terms(
        kept_input_rows, norm_gain_vector
    )
    stacked = jnp.concatenate([normed_kept_rows, normed_later], axis=0)
    up_whole = lax.all_gather(up_weight, "fs", axis=0, tiled=True)
    down_whole = lax.all_gather(down_weight, "fs", axis=1, tiled=True)
    pre_act = jnp.dot(stacked, up_whole, preferred_element_type=jnp.float32)
    pre_saved = pre_act[:row_count]
    hidden_saved = squared_relu(pre_saved)
    hidden_later = squared_relu(pre_act[row_count:])
    mixed_part = jnp.dot(hidden_later, down_whole, preferred_element_type=jnp.float32)
    hidden_grad = lax.dot_general(
        cotangent, down_whole, TRANSPOSED, preferred_element_type=jnp.float32
    )
    pre_grad = (hidden_grad * 2.0 * jax.nn.relu(pre_saved)).astype(jnp.bfloat16)
    back_part = lax.dot_general(pre_grad, up_whole, TRANSPOSED, preferred_element_type=jnp.float32)
    mixed_sum, back_sum = (
        lax.psum(mixed_part.astype(jnp.bfloat16), "tp").astype(jnp.float32),
        lax.psum(back_part.astype(jnp.bfloat16), "tp").astype(jnp.float32),
    )
    mixed = mixed_sum.astype(jnp.bfloat16)
    scaled_rows = back_sum * norm_gain_vector
    input_gradient_rows = (
        inverse_rms_kept
        * (
            scaled_rows
            - unit_kept_rows * jnp.mean(scaled_rows * unit_kept_rows, axis=-1, keepdims=True)
        )
    ).astype(jnp.bfloat16)
    cot_columns, normed_columns = (
        lax.all_to_all(cotangent, "fs", split_axis=1, concat_axis=0, tiled=True),
        lax.all_to_all(normed_kept_rows, "fs", split_axis=1, concat_axis=0, tiled=True),
    )
    columns = normed_columns
    up_grad = grad_scale * lax.dot_general(
        columns,
        lax.all_gather(pre_grad, "fs", axis=0, tiled=True),
        LEADING,
        preferred_element_type=jnp.float32,
    )
    columns = cot_columns
    down_grad = lax.dot_general(
        lax.all_gather(hidden_saved, "fs", axis=0, tiled=True),
        columns,
        LEADING,
        preferred_element_type=jnp.float32,
    )
    up_added, down_added = (
        lax.psum(up_grad.astype(jnp.bfloat16), "rep").astype(jnp.float32),
        lax.psum((down_grad * grad_scale).astype(jnp.bfloat16), "rep").astype(jnp.float32),
    )
    return (mixed, input_gradient_rows, up_sum + up_added, down_sum + down_added)

def layer_kernel(
    n_fs, grad_scale, x_ref, kept_ref, cot_ref, gain_ref, up_ref, down_ref,
    mixed_out, input_out, up_out, down_out,
    kept, fresh, tok, up_own, down_own, up_pass, down_pass, pre_kept, hidden, pre_grad,
    grad_kept, grad_sent, grad_got, grad_sum, grad_line, grad_pair, grad_all,
    part, got_first, got_second, got_third, rows_out,
    load_sem, pair_send, pair_recv, line_send, line_recv, core_send, core_recv, own_sem,
    tok_send, tok_recv, share_send, share_recv, gline_send, gline_recv,
    gpair_send, gpair_recv, grep_send, grep_recv, part_send, part_recv, out_send, out_recv,
):
    rep, fs, core = lax.axis_index("rep"), lax.axis_index("fs"), lax.axis_index("tp")
    outer = n_fs // 2
    place, pair = fs // 2, fs % 2
    low = place % 2
    rows, width = tok.shape[2:]
    depth, own = up_pass.shape
    n_slots = tok.shape[1]
    tokens = n_slots * rows
    other_core = (rep, fs, 1 - core)
    start_row = pl.multiple_of(core * rows, rows)

    def place_at(step):
        return (place, place + 1 - 2 * low, (place + 2) % outer, outer - 1 - place)[step]

    def line_peer(step):
        return (rep, place_at(step) * 2 + pair, core)

    def partner(dim):
        if dim == X:
            return (1 - rep, fs, core)
        if dim == Y:
            return (rep, place * 2 + 1 - pair, core)
        return line_peer(1)

    def flip(bit, on):
        return 1 - bit if on else bit

    def slot(mask):
        return flip(rep, mask & X) * 4 + flip(pair, mask & Y) * 2 + flip(low, mask & Z)

    def block(rep_at, pair_at, low_at):
        return (rep_at * 2 + pair_at) * 2 + low_at

    def copy(source, target, send, recv, device):
        return pltpu.make_async_remote_copy(
            src_ref=source, dst_ref=target, send_sem=send, recv_sem=recv,
            device_id=device, device_id_type=MESH,
        )

    sent = []

    def go(source, target, send, recv, device):
        one = copy(source, target, send, recv, device)
        one.start()
        sent.append(one)

    seen = set()

    def landed(target, sem, *name):
        if name not in seen:
            seen.add(name)
            copy(target, target, sem, sem, other_core).wait_recv()

    own_rows = pl.ds(start_row, rows)
    loads = [
        pltpu.make_async_copy(kept_ref.at[own_rows, :], kept, load_sem.at[0]),
        pltpu.make_async_copy(x_ref.at[own_rows, :], fresh, load_sem.at[1]),
        pltpu.make_async_copy(cot_ref.at[own_rows, :], tok.at[COT, slot(0)], load_sem.at[2]),
    ]
    for one in loads:
        one.start()
    barrier = pltpu.get_barrier_semaphore()
    peers = [other_core, partner(X), partner(Y)] + [line_peer(step) for step in range(1, outer)]
    for peer in peers:
        pl.semaphore_signal(barrier, inc=1, device_id=peer, device_id_type=MESH)

    for one in loads:
        one.wait()
    gain = gain_ref[...]
    tok[SAVED, slot(0)] = norm_partial_terms(kept[...], gain)[2]
    tok[LATER, slot(0)] = norm_partial_terms(fresh[...], gain)[2]
    pl.semaphore_wait(barrier, len(peers))

    def up_source(index):
        return up_ref.at[:, pl.ds(pl.multiple_of(index * own, own), own)]

    def down_source(index):
        return down_ref.at[pl.ds(pl.multiple_of(index * own, own), own), :]

    def up_slot(half, place_to, pair_to, count=1):
        first = pl.multiple_of((place_to * 2 + pair_to) * depth, depth)
        return up_own.at[half, pl.ds(first, count * depth), :]

    def down_slot(half, place_to, pair_to, count=1):
        first = pl.multiple_of((place_to * 2 + pair_to) * depth, depth)
        return down_own.at[half, :, pl.ds(first, count * depth)]

    def tok_landed(array, mask):
        landed(tok.at[array, slot(mask)], tok_recv.at[array, mask - 1], TOKENS, array, mask)

    tok_counts = [0, 0, 0]

    def send_tok(array, mask, dim):
        if mask:
            tok_landed(array, mask)
        at = tok.at[array, slot(mask)]
        number = tok_counts[array]
        tok_counts[array] += 1
        go(at, at, tok_send.at[array, number], tok_recv.at[array, (mask ^ dim) - 1], partner(dim))

    def tok_end(array):
        for mask in range(1, n_slots):
            tok_landed(array, mask)

    sides = (UP, DOWN)
    source_of = (up_source, down_source)
    slot_of = (up_slot, down_slot)
    pass_of = (up_pass, down_pass)
    steps = (1, 3, 2)

    def pair_begin(kind):
        for which, low_to in enumerate((low, 1 - low)):
            target = pass_of[kind] if which else slot_of[kind](core, place, pair)
            go(
                source_of[kind](block(rep, 1 - pair, low_to)), target,
                pair_send.at[which, kind], pair_recv.at[which, kind], partner(Y),
            )

    def line_begin(kind):
        for step in steps:
            go(
                source_of[kind](block(rep, pair, flip(low, step % 2))), slot_of[kind](core, place, pair),
                line_send.at[step - 1, 0, kind], line_recv.at[step - 1, 0, kind], line_peer(step),
            )

    def pair_end(kind):
        landed(slot_of[kind](core, place, 1 - pair), pair_recv.at[0, kind], PAIR, kind, 0)
        landed(pass_of[kind], pair_recv.at[1, kind], PAIR, kind, 1)

    def line_pass(kind):
        pair_end(kind)
        near = slot_of[kind](core, place, 1 - pair)
        for step in steps:
            go(
                pass_of[kind] if step % 2 else near, near,
                line_send.at[step - 1, 1, kind], line_recv.at[step - 1, 1, kind], line_peer(step),
            )

    def line_landed(kind, step):
        for number, pair_at in enumerate((pair, 1 - pair)):
            landed(
                slot_of[kind](core, place_at(step), pair_at), line_recv.at[step - 1, number, kind],
                LINE, kind, step, number,
            )

    def own_end(kind):
        pair_end(kind)
        if (OWN, kind) not in seen:
            seen.add((OWN, kind))
            keep[kind].wait()

    def to_core(kind, step):
        if step:
            line_landed(kind, step)
        else:
            own_end(kind)
        mine = slot_of[kind](core, place_at(step), 0, 2)
        go(mine, mine, core_send.at[step, kind], core_recv.at[step, kind], other_core)

    def weights_end(kind, number):
        if number:
            for step in range(outer):
                target = slot_of[kind](1 - core, place_at(step), 0, 2)
                landed(target, core_recv.at[step, kind], CORE, kind, step)
        else:
            own_end(kind)
            for step in range(1, outer):
                line_landed(kind, step)

    keep = [
        pltpu.make_async_copy(
            source_of[kind](block(rep, pair, low)), slot_of[kind](core, place, pair), own_sem.at[kind]
        )
        for kind in sides
    ]

    def all_tokens(array):
        return tok[array].reshape(tokens, width)

    def saved_pre(number):
        half = (core, 1 - core)[number]
        tok_end(SAVED)
        weights_end(UP, number)
        pre = jnp.dot(all_tokens(SAVED), up_own[half], preferred_element_type=jnp.float32)
        pre_kept[half] = jax.nn.relu(pre)
        hidden[half] = squared_relu(pre)

    def saved_grad(number):
        half = (core, 1 - core)[number]
        tok_end(COT)
        weights_end(DOWN, number)
        grad = lax.dot_general(
            all_tokens(COT), down_own[half], TRANSPOSED, preferred_element_type=jnp.float32
        )
        pre_grad[half] = (grad * 2.0 * pre_kept[half]).astype(jnp.bfloat16)

    chunk = width // outer

    def chunk_at(index):
        return pl.ds(pl.multiple_of(index * chunk, chunk), chunk)

    def weight_grad(kind, half, columns):
        left = hidden[half] if kind == DOWN else pre_grad[half]
        right = tok[COT if kind == DOWN else SAVED, :, :, columns].reshape(tokens, chunk)
        return grad_scale * lax.dot_general(left, right, LEADING, preferred_element_type=jnp.float32)

    def grad_share(kind):
        if kind == DOWN:
            tok_end(COT)

        @pl.loop(0, outer)
        def _(index):
            columns = chunk_at(index)
            grad_sent[kind, :, columns] = weight_grad(kind, 1 - core, columns).astype(jnp.bfloat16)

        go(grad_sent.at[kind], grad_got.at[kind], share_send.at[kind], share_recv.at[kind], other_core)

    def grad_keep(kind):
        if kind == DOWN:
            tok_end(COT)

        @pl.loop(0, outer)
        def _(index):
            columns = chunk_at(index)
            grad_kept[kind, :, columns] = weight_grad(kind, core, columns)

    def grad_begin(kind):
        landed(grad_got.at[kind], share_recv.at[kind], SHARE, kind)

        @pl.loop(0, outer)
        def _(index):
            columns = chunk_at(index)
            grad_sum[kind, :, columns] = (
                grad_kept[kind, :, columns] + grad_got[kind, :, columns].astype(jnp.float32)
            ).astype(jnp.bfloat16)

        for number, pair_at in enumerate((1 - pair, pair)):
            for step in steps:
                columns = pl.ds(pl.multiple_of((place_at(step) * 2 + pair_at) * depth, depth), depth)
                go(
                    grad_sum.at[kind, :, columns], grad_line.at[step - 1, kind, number],
                    gline_send.at[step - 1, kind, number], gline_recv.at[step - 1, kind, number],
                    line_peer(step),
                )

    def part_at(array, side, mask):
        return part.at[array, slot(mask), side]

    def part_first(array, side, number):
        first, second = SUM_ORDERS[array][side]
        for place_in in (2 * number, 2 * number + 1):
            mask = (second | Z, second, Z, 0)[place_in]
            go(
                part_at(array, side, first | mask), got_first.at[array, side, place_in],
                part_send.at[array, side, place_in], part_recv.at[array, side, place_in], partner(first),
            )

    def part_landed(array, side, number):
        got = got_first.at[array, side, number] if number < 4 else (
            got_second.at[array, side, number - 4] if number < 6 else got_third.at[array, side]
        )
        landed(got, part_recv.at[array, side, number], PARTS, array, side, number)
        return got

    def part_add(array, side, mask, *got):
        total = part_at(array, side, mask)[...].astype(jnp.float32)
        for one in got:
            total = total + one[...].astype(jnp.float32)
        return total

    def part_second(array, side, number):
        first, second = SUM_ORDERS[array][side]
        mask = (second | Z, second)[number]
        got = part_landed(array, side, number)
        at = part_at(array, side, mask)
        at[...] = part_add(array, side, mask, got).astype(jnp.bfloat16)
        go(
            at, got_second.at[array, side, number],
            part_send.at[array, side, 4 + number], part_recv.at[array, side, 4 + number], partner(second),
        )

    def part_third(array, side):
        got = [part_landed(array, side, number) for number in (2, 4)]
        at = part_at(array, side, Z)
        at[...] = part_add(array, side, Z, *got).astype(jnp.bfloat16)
        go(
            at, got_third.at[array, side],
            part_send.at[array, side, 6], part_recv.at[array, side, 6], partner(Z),
        )

    def part_last(array, side):
        return part_add(array, side, 0, *[part_landed(array, side, number) for number in (3, 5, 6)])

    def back_sums():
        @pl.loop(0, outer)
        def _(index):
            columns = chunk_at(index)
            total = jnp.zeros((tokens, chunk), jnp.float32)
            for half in range(2):
                total = total + lax.dot_general(
                    pre_grad[half], up_own[half, columns, :], TRANSPOSED,
                    preferred_element_type=jnp.float32,
                )
            part[BACK, :, :, :, columns] = total.astype(jnp.bfloat16).reshape(n_slots, 2, rows // 2, chunk)

    def mixed_sums():
        tok_end(LATER)

        @pl.loop(0, 2)
        def _(half):
            hidden[half] = squared_relu(
                jnp.dot(all_tokens(LATER), up_own[half], preferred_element_type=jnp.float32)
            )

        @pl.loop(0, outer)
        def _(index):
            columns = chunk_at(index)
            total = jnp.zeros((tokens, chunk), jnp.float32)
            for half in range(2):
                total = total + jnp.dot(
                    hidden[half], down_own[half, :, columns], preferred_element_type=jnp.float32
                )
            part[MIXED, :, :, :, columns] = total.astype(jnp.bfloat16).reshape(n_slots, 2, rows // 2, chunk)

    def line_part(kind, which, number):
        if which:
            total = grad_line[0, kind, number].astype(jnp.float32)
            total = total + grad_line[2, kind, number].astype(jnp.float32)
        else:
            pair_at = (1 - pair, pair)[number]
            mine = pl.ds(pl.multiple_of((place * 2 + pair_at) * depth, depth), depth)
            total = grad_sum[kind, :, mine].astype(jnp.float32)
            total = total + grad_line[1, kind, number].astype(jnp.float32)
        return (total.T if kind == UP else total).astype(jnp.bfloat16)

    def blocks_at(kind, rep_at, pair_at):
        return grad_all.at[kind, pl.ds(block(rep_at, pair_at, 0), 2)]

    def grad_spread(kind, number):
        for step in steps:
            landed(
                grad_line.at[step - 1, kind, number], gline_recv.at[step - 1, kind, number],
                GRAD_LINE, kind, step, number,
            )
        for which, low_at in enumerate((low, 1 - low)):
            if number:
                grad_all[kind, block(rep, pair, low_at)] = line_part(kind, which, number)
            else:
                grad_pair[kind, low_at] = line_part(kind, which, number)
        mine = blocks_at(kind, rep, pair)
        if number:
            go(mine, mine, grep_send.at[kind, 0], grep_recv.at[kind, 0], partner(X))
            grad_out(kind, rep, pair)
        else:
            go(grad_pair.at[kind], mine, gpair_send.at[kind], gpair_recv.at[kind], partner(Y))

    def grad_pass(kind):
        near = blocks_at(kind, rep, 1 - pair)
        landed(near, gpair_recv.at[kind], GRAD_PAIR, kind)
        go(near, near, grep_send.at[kind, 1], grep_recv.at[kind, 1], partner(X))
        grad_out(kind, rep, 1 - pair)

    def grad_out(kind, rep_at, pair_at):
        for low_at in range(2):
            index = block(rep_at, pair_at, low_at)
            place_to = pl.ds(pl.multiple_of(index * own, own), own)
            if kind == UP:
                up_out[:, place_to] = grad_all[UP, index]
            else:
                down_out[place_to, :] = grad_all[DOWN, index]

    def grad_end(kind, number):
        pair_at = (pair, 1 - pair)[number]
        landed(blocks_at(kind, 1 - rep, pair_at), grep_recv.at[kind, number], GRAD_REP, kind, number)
        grad_out(kind, 1 - rep, pair_at)

    def share_rows(array):
        mine = rows_out.at[array, core]
        go(mine, mine, out_send.at[array], out_recv.at[array], other_core)

    def back_end():
        for side in range(2):
            scaled_rows = part_last(BACK, side) * gain
            at = pl.ds(side * (rows // 2), rows // 2)
            inverse, unit_rows, _ = norm_partial_terms(kept[at, :], gain)
            rows_out[BACK, core, side] = (
                inverse
                * (scaled_rows - unit_rows * jnp.mean(scaled_rows * unit_rows, axis=-1, keepdims=True))
            ).astype(jnp.bfloat16)
        share_rows(BACK)

    def mixed_end():
        for side in range(2):
            rows_out[MIXED, core, side] = part_last(MIXED, side).astype(jnp.bfloat16)
        share_rows(MIXED)

    def rows_end(array, out):
        landed(rows_out.at[array, 1 - core], out_recv.at[array], ROWS, array)
        out[...] = rows_out[array].reshape(2 * rows, width)

    def finish():
        for kind in KIND_ORDER:
            for number in range(2):
                grad_end(kind, number)
        rows_end(BACK, input_out)
        rows_end(MIXED, mixed_out)

    for one in keep:
        one.start()
    ends = (back_end, mixed_end)
    jobs = {
        TOK: send_tok, PAIR: pair_begin, LINE: line_begin, LINE_PASS: line_pass, CORE: to_core,
        PRE: saved_pre, GRAD: saved_grad, SHARE: grad_share, KEEP: grad_keep, GRAD_LINE: grad_begin,
        GRAD_PAIR: grad_spread, GRAD_REP: grad_pass, BACK_SUMS: back_sums, MIXED_SUMS: mixed_sums,
        FIRST: part_first, SECOND: part_second, THIRD: part_third, LAST: lambda array: ends[array](),
        END: finish,
    }
    for job, *details in SCHEDULE:
        jobs[job](*details)
    for one in sent:
        one.wait_send()


def cube_body(
    x_later, kept_input_rows, cotangent, norm_gain_vector, up_weight, down_weight, up_sum, down_sum
):
    row_count, width = x_later.shape
    n_fs = lax.axis_size("fs")
    grad_scale = float(row_count * lax.axis_size("rep") * n_fs) ** (-0.5)
    depth, units = up_weight.shape
    own = units // n_fs
    rows = row_count // 2
    outer = n_fs // 2
    tokens = n_fs * rows
    kind = x_later.dtype
    dma = pltpu.SemaphoreType.DMA
    vmem = functools.partial(pltpu.VMEM, dtype=kind)
    inside = pl.BlockSpec(memory_space=pltpu.VMEM)
    outside = pl.BlockSpec(memory_space=pltpu.HBM)
    mixed, input_gradient_rows, up_added, down_added = pl.pallas_call(
        functools.partial(layer_kernel, n_fs, grad_scale),
        out_shape=(
            jax.ShapeDtypeStruct((row_count, width), kind),
            jax.ShapeDtypeStruct((row_count, width), kind),
            jax.ShapeDtypeStruct((depth, units), kind),
            jax.ShapeDtypeStruct((units, depth), kind),
        ),
        in_specs=[outside] * 3 + [inside] + [outside] * 2,
        out_specs=[inside] * 4,
        scratch_shapes=[
            vmem((rows, width)), vmem((rows, width)), vmem((3, n_fs, rows, width)),
            vmem((2, width, own)), vmem((2, own, width)), vmem((depth, own)), vmem((own, depth)),
            pltpu.VMEM((2, tokens, own), jnp.float32), vmem((2, tokens, own)), vmem((2, tokens, own)),
            pltpu.VMEM((2, own, width), jnp.float32),
            vmem((2, own, width)), vmem((2, own, width)), vmem((2, own, width)),
            vmem((3, 2, 2, own, depth)), vmem((2, 2, own, depth)), vmem((2, n_fs, own, depth)),
            vmem((2, n_fs, 2, rows // 2, width)),
            vmem((2, 2, 4, rows // 2, width)), vmem((2, 2, 2, rows // 2, width)),
            vmem((2, 2, rows // 2, width)), vmem((2, 2, 2, rows // 2, width)),
            dma((3,)), dma((2, 2)), dma((2, 2)), dma((3, 2, 2)), dma((3, 2, 2)), dma((outer, 2)), dma((outer, 2)),
            dma((2,)), dma((3, 7)), dma((3, 7)), dma((2,)), dma((2,)), dma((3, 2, 2)), dma((3, 2, 2)),
            dma((2,)), dma((2,)), dma((2, 2)), dma((2, 2)), dma((2, 2, 7)), dma((2, 2, 7)), dma((2,)), dma((2,)),
        ],
        compiler_params=pltpu.CompilerParams(
            collective_id=0, has_side_effects=True, vmem_limit_bytes=VMEM_BYTES
        ),
    )(
        x_later, kept_input_rows, cotangent, norm_gain_vector.reshape(1, width), up_weight, down_weight,
    )
    return (
        mixed,
        input_gradient_rows,
        up_sum + up_added.astype(jnp.float32),
        down_sum + down_added.astype(jnp.float32),
    )


def chosen_body(*args):
    depth, units = args[4].shape
    n_fs = lax.axis_size("fs")
    cubes = lax.axis_size("tp") == 2 and lax.axis_size("rep") == 2 and n_fs == 8
    return (cube_body if cubes and units == depth * n_fs and depth % 128 == 0 else body)(*args)


def solution(mesh):
    return jax.shard_map(
        chosen_body,
        mesh=mesh,
        in_specs=(
            P(("rep", "fs"), None),
            P(("rep", "fs"), None),
            P(("rep", "fs"), None),
            P(),
            P("fs", "tp"),
            P("tp", "fs"),
            P("fs", "tp"),
            P("tp", "fs"),
        ),
        out_specs=(P(("rep", "fs"), None), P(("rep", "fs"), None), P("fs", "tp"), P("tp", "fs")),
        check_vma=False,
    )
```

time: 157 us -> 136 us (0.87)
  Pallas kernels: 149 us -> 127 us
    pallas_call x1, Pallas kernels: 149 us -> 127 us  [cube_body(): pl.pallas_call(functools.partial(layer_kernel, n_fs, grad_scale), out_sha...]
where the time goes in v2:
time: 136 us; the launch traced here: 134 us
  Pallas kernels  127 us (93%)
  other arithmetic  5.22 us (4%)
  local copies, waits for them, and re-layouts  1.6 us (1%)
    pallas_call x1, Pallas kernels, cube_body(): pl.pallas_call(functools.partial(layer_kernel, n_fs, grad_scale), out_sha...  127 us
    add x1, other arithmetic, cube_body(): up_sum + up_added.astype(jnp.float32)  3.7 us

profile of v2, /device:TPU:0, one launch (start us, length us, event | category | flops | bytes accessed | tf_op | source)
XLA Modules:
  0.0 134.0 jit_solution(4656136512973012877)
XLA Ops:
  0.6 126.6 %shard_map.111 = (bf16[128,2048]{1,0:T(8,128)(2,1)}, bf16[128,2048]{1,0:T(8,128)(2,1)}, bf16[256,2048]{1,0:T(8,128)(2,1)}, bf16[2048,256]{1,0:T(8,128)(2,1)}) custom-call(bf16[128,2048]{1,0:T(8,128)(2,1)} %x_ref.1, bf16[128,2048]{1,0:T(8,128)(2,1)} %kept_ref.1, bf16[128,2048]{1,0:T(8,128)(2,1)} %cot_ref.1, f32[1,2048]{1,0:T(1,128)} %bitcast.1, ...), custom_call_target="tpu_custom_call" | custom-call | tf_op jit(solution)/shard_map/pallas_call | solution.py:563
  127.2 0.0 copy-start
  127.2 0.0 copy-start.1
  127.2 3.7 %convert_add_fusion.1 = f32[256,2048]{1,0:T(8,128)} fusion(f32[256,2048]{1,0:T(8,128)} %param.14, bf16[256,2048]{1,0:T(8,128)(2,1)} %get-tuple-element.10), kind=kLoop, calls=%fused_computation.1 | loop fusion | flops 1048576 | bytes 5242880 | tf_op jit(solution)/shard_map/add | solution.py:596
  130.9 0.0 copy-done
  130.9 0.0 copy-done.1
  130.9 0.0 copy-start.3
  130.9 0.0 copy-start.2
  130.9 1.5 %convert_add_fusion = f32[2048,256]{1,0:T(8,128)} fusion(f32[2048,256]{1,0:T(8,128)S(1)} %copy-done, bf16[2048,256]{1,0:T(8,128)(2,1)S(1)} %copy-done.1), kind=kLoop, calls=%fused_computation | loop fusion | flops 1048576 | bytes 5242880 | tf_op jit(solution)/shard_map/add | solution.py:597
  132.5 0.0 copy-done.3
  132.5 0.8 copy.14
  133.3 0.0 copy-done.2
  133.3 0.8 copy.15
Async XLA Ops:
  127.2 3.7 %copy-start = (f32[2048,256]{1,0:T(8,128)S(1)}, f32[2048,256]{1,0:T(8,128)}, u32[]{:S(2)}) copy-start(f32[2048,256]{1,0:T(8,128)} %param.15) | copy-start | bytes 6291460
  127.2 3.7 %copy-start.1 = (bf16[2048,256]{1,0:T(8,128)(2,1)S(1)}, bf16[2048,256]{1,0:T(8,128)(2,1)}, u32[]{:S(2)}) copy-start(bf16[2048,256]{1,0:T(8,128)(2,1)} %get-tuple-element.11) | copy-start | bytes 3145732
  130.9 1.5 %copy-start.3 = (bf16[128,2048]{1,0:T(8,128)(2,1)S(1)}, bf16[128,2048]{1,0:T(8,128)(2,1)}, u32[]{:S(2)}) copy-start(bf16[128,2048]{1,0:T(8,128)(2,1)} %get-tuple-element.16) | copy-start | bytes 1572868
  130.9 2.3 %copy-start.2 = (bf16[128,2048]{1,0:T(8,128)(2,1)S(1)}, bf16[128,2048]{1,0:T(8,128)(2,1)}, u32[]{:S(2)}) copy-start(bf16[128,2048]{1,0:T(8,128)(2,1)} %get-tuple-element.17) | copy-start | bytes 1572868

commit v3 on v2

--- a/solution.py
+++ b/solution.py
@@ -18,26 +18,31 @@
 (TOK, PAIR, LINE, LINE_PASS, CORE, PRE, GRAD, SHARE, KEEP, GRAD_LINE,
  GRAD_PAIR, GRAD_REP, BACK_SUMS, MIXED_SUMS, FIRST, SECOND, THIRD, LAST, END, TOKENS, OWN, PARTS, ROWS) = range(23)
 KIND_ORDER = (DOWN, UP)
-SUM_ORDERS = (((X, Y), (Y, X)), ((X, Y), (Y, X)))
+TOKEN_ORDERS = (((Z, X, Y), (Z, Y, X)), ((Z, Y, X), (Z, Y, X)), ((Z, X, Y), (Z, Y, X)))
+SUM_ORDERS = (((Y, X, Z), (X, Y, Z)), ((Y, X, Z), (Y, X, Z)))
 SCHEDULE = (
-    (TOK, COT, 0, Y), (PAIR, UP), (TOK, COT, 0, X), (TOK, SAVED, 0, Y), (TOK, LATER, 0, X),
-    (TOK, SAVED, 0, Z), (LINE, UP), (TOK, SAVED, 0, X), (TOK, COT, Y, X), (TOK, COT, 0, Z),
-    (TOK, SAVED, Z, Y), (PAIR, DOWN), (LINE_PASS, UP), (TOK, SAVED, Z, X), (TOK, SAVED, Y, X),
-    (TOK, LATER, 0, Y), (TOK, COT, Z, Y), (CORE, UP, 0), (TOK, LATER, 0, Z), (LINE_PASS, DOWN),
-    (TOK, COT, Z, X), (TOK, LATER, X, Y), (LINE, DOWN), (CORE, UP, 2), (CORE, UP, 3),
-    (CORE, DOWN, 0), (CORE, UP, 1), (TOK, SAVED, Y | Z, X), (TOK, COT, Y | Z, X),
-    (TOK, LATER, Z, X), (PRE, 1), (TOK, LATER, Z, Y), (PRE, 0), (CORE, DOWN, 1), (KEEP, DOWN),
-    (SHARE, DOWN), (CORE, DOWN, 3), (CORE, DOWN, 2), (GRAD_LINE, DOWN), (GRAD, 0), (GRAD, 1),
-    (BACK_SUMS,), (FIRST, BACK, 0, 0), (TOK, LATER, X | Z, Y), (FIRST, BACK, 0, 1),
-    (FIRST, BACK, 1, 0), (MIXED_SUMS,), (SECOND, BACK, 1, 0), (KEEP, UP), (FIRST, MIXED, 0, 0),
-    (SECOND, BACK, 0, 1), (FIRST, MIXED, 0, 1), (SHARE, UP), (GRAD_PAIR, DOWN, 0),
-    (FIRST, MIXED, 1, 1), (SECOND, BACK, 0, 0), (SECOND, MIXED, 0, 0), (GRAD_LINE, UP),
-    (FIRST, MIXED, 1, 0), (FIRST, BACK, 1, 1), (GRAD_REP, DOWN), (GRAD_PAIR, DOWN, 1),
-    (THIRD, BACK, 0), (THIRD, MIXED, 0), (SECOND, BACK, 1, 1), (SECOND, MIXED, 1, 0),
-    (SECOND, MIXED, 1, 1), (GRAD_PAIR, UP, 0), (GRAD_PAIR, UP, 1), (THIRD, BACK, 1), (GRAD_REP, UP),
-    (THIRD, MIXED, 1), (SECOND, MIXED, 0, 1), (LAST, BACK), (LAST, MIXED), (END,),
+    (TOK, COT, 1, 1), (TOK, COT, 0, 0), (TOK, COT, 0, 1), (TOK, SAVED, 0, 2), (TOK, SAVED, 1, 1),
+    (TOK, SAVED, 1, 0), (TOK, LATER, 0, 1), (LINE, UP), (TOK, LATER, 1, 1), (TOK, COT, 1, 5),
+    (TOK, SAVED, 1, 2), (PAIR, UP), (TOK, COT, 1, 2), (TOK, SAVED, 0, 0), (CORE, UP, 0),
+    (TOK, COT, 1, 0), (TOK, SAVED, 0, 1), (TOK, LATER, 0, 0), (LINE_PASS, UP), (TOK, LATER, 1, 5),
+    (TOK, SAVED, 0, 3), (TOK, COT, 0, 4), (LINE, DOWN), (TOK, SAVED, 1, 4), (TOK, SAVED, 1, 3),
+    (TOK, LATER, 1, 0), (TOK, COT, 0, 3), (TOK, COT, 0, 5), (TOK, SAVED, 0, 5), (TOK, SAVED, 1, 5),
+    (PAIR, DOWN), (TOK, COT, 1, 3), (TOK, SAVED, 1, 6), (TOK, SAVED, 0, 4), (CORE, UP, 2),
+    (TOK, COT, 0, 2), (CORE, UP, 1), (TOK, SAVED, 0, 6), (TOK, COT, 0, 6), (CORE, UP, 3),
+    (TOK, COT, 1, 6), (CORE, DOWN, 0), (TOK, COT, 1, 4), (TOK, LATER, 0, 4), (LINE_PASS, DOWN),
+    (TOK, LATER, 0, 5), (TOK, LATER, 1, 3), (TOK, LATER, 1, 2), (TOK, LATER, 0, 2), (PRE, 1),
+    (PRE, 0), (SHARE, DOWN), (TOK, LATER, 0, 3), (TOK, LATER, 1, 4), (KEEP, DOWN),
+    (GRAD_LINE, DOWN), (CORE, DOWN, 1), (CORE, DOWN, 3), (TOK, LATER, 0, 6), (CORE, DOWN, 2),
+    (GRAD, 0), (TOK, LATER, 1, 6), (GRAD, 1), (BACK_SUMS,), (FIRST, BACK, 1, 1),
+    (FIRST, BACK, 0, 1), (KEEP, UP), (SHARE, UP), (FIRST, BACK, 1, 0), (FIRST, BACK, 0, 0),
+    (SECOND, BACK, 0, 0), (GRAD_PAIR, DOWN, 0), (SECOND, BACK, 0, 1), (MIXED_SUMS,),
+    (FIRST, MIXED, 0, 0), (GRAD_LINE, UP), (FIRST, MIXED, 0, 1), (GRAD_PAIR, DOWN, 1),
+    (FIRST, MIXED, 1, 0), (GRAD_REP, DOWN), (SECOND, MIXED, 0, 1), (SECOND, BACK, 1, 0),
+    (SECOND, MIXED, 1, 0), (SECOND, MIXED, 0, 0), (GRAD_PAIR, UP, 0), (SECOND, MIXED, 1, 1),
+    (THIRD, BACK, 1), (GRAD_PAIR, UP, 1), (THIRD, BACK, 0), (FIRST, MIXED, 1, 1), (THIRD, MIXED, 0),
+    (GRAD_REP, UP), (THIRD, MIXED, 1), (SECOND, BACK, 1, 1), (LAST, MIXED), (LAST, BACK), (END,),
 )
-VMEM_BYTES = 64 * 2**20 - 2**16
+VMEM_BYTES = 48 * 2**20
 
 
 def norm_partial_terms(values, norm_gain_vector):
@@ -112,20 +117,22 @@
     return (mixed, input_gradient_rows, up_sum + up_added, down_sum + down_added)
 
 def layer_kernel(
-    n_fs, grad_scale, x_ref, kept_ref, cot_ref, gain_ref, up_ref, down_ref,
+    n_fs, grad_scale, x_ref, kept_ref, cot_ref, gain_ref, up_ref, down_ref, up_sum_ref, down_sum_ref,
     mixed_out, input_out, up_out, down_out,
-    kept, fresh, tok, up_own, down_own, up_pass, down_pass, pre_kept, hidden, pre_grad,
+    gain_kept, kept, fresh, tok, up_own, down_own, up_pass, down_pass, pre_kept, hidden, pre_grad,
     grad_kept, grad_sent, grad_got, grad_sum, grad_line, grad_pair, grad_all,
-    part, got_first, got_second, got_third, rows_out,
+    part, got_first, got_second, got_third, rows_out, up_total, down_total,
     load_sem, pair_send, pair_recv, line_send, line_recv, core_send, core_recv, own_sem,
-    tok_send, tok_recv, share_send, share_recv, gline_send, gline_recv,
-    gpair_send, gpair_recv, grep_send, grep_recv, part_send, part_recv, out_send, out_recv,
+    tok_send, tok_recv, tok_last, share_send, share_recv, gline_send, gline_recv,
+    gpair_send, gpair_recv, grep_send, grep_recv, part_send, part_recv, part_end,
+    out_send, out_recv, sum_sem, store_sem,
 ):
     rep, fs, core = lax.axis_index("rep"), lax.axis_index("fs"), lax.axis_index("tp")
     outer = n_fs // 2
     place, pair = fs // 2, fs % 2
     low = place % 2
-    rows, width = tok.shape[2:]
+    half_rows, width = tok.shape[3:]
+    rows = 2 * half_rows
     depth, own = up_pass.shape
     n_slots = tok.shape[1]
     tokens = n_slots * rows
@@ -160,12 +167,14 @@
             device_id=device, device_id_type=MESH,
         )
 
-    sent = []
+    def reached(order, reach):
+        return sum(dim for step, dim in enumerate(order) if reach >> step & 1)
 
     def go(source, target, send, recv, device):
-        one = copy(source, target, send, recv, device)
-        one.start()
-        sent.append(one)
+        copy(source, target, send, recv, device).start()
+
+    def all_sent(source, sem):
+        copy(source, source, sem, sem, other_core).wait_send()
 
     seen = set()
 
@@ -178,7 +187,16 @@
     loads = [
         pltpu.make_async_copy(kept_ref.at[own_rows, :], kept, load_sem.at[0]),
         pltpu.make_async_copy(x_ref.at[own_rows, :], fresh, load_sem.at[1]),
-        pltpu.make_async_copy(cot_ref.at[own_rows, :], tok.at[COT, slot(0)], load_sem.at[2]),
+    ]
+    loads += [
+        pltpu.make_async_copy(
+            cot_ref.at[pl.ds(pl.multiple_of(start_row + side * half_rows, half_rows), half_rows), :],
+            tok.at[COT, slot(0), side], load_sem.at[2 + side],
+        )
+        for side in range(2)
+    ]
+    loads += [
+        pltpu.make_async_copy(gain_ref, gain_kept, load_sem.at[4]),
     ]
     for one in loads:
         one.start()
@@ -189,9 +207,10 @@
 
     for one in loads:
         one.wait()
-    gain = gain_ref[...]
-    tok[SAVED, slot(0)] = norm_partial_terms(kept[...], gain)[2]
-    tok[LATER, slot(0)] = norm_partial_terms(fresh[...], gain)[2]
+    gain = gain_kept[...]
+    own_shape = (2, half_rows, width)
+    tok[SAVED, slot(0)] = norm_partial_terms(kept[...], gain)[2].reshape(own_shape)
+    tok[LATER, slot(0)] = norm_partial_terms(fresh[...], gain)[2].reshape(own_shape)
     pl.semaphore_wait(barrier, len(peers))
 
     def up_source(index):
@@ -208,22 +227,24 @@
         first = pl.multiple_of((place_to * 2 + pair_to) * depth, depth)
         return down_own.at[half, :, pl.ds(first, count * depth)]
 
-    def tok_landed(array, mask):
-        landed(tok.at[array, slot(mask)], tok_recv.at[array, mask - 1], TOKENS, array, mask)
-
-    tok_counts = [0, 0, 0]
-
-    def send_tok(array, mask, dim):
-        if mask:
-            tok_landed(array, mask)
-        at = tok.at[array, slot(mask)]
-        number = tok_counts[array]
-        tok_counts[array] += 1
-        go(at, at, tok_send.at[array, number], tok_recv.at[array, (mask ^ dim) - 1], partner(dim))
+    def tok_landed(array, side, reach):
+        mask = reached(TOKEN_ORDERS[array][side], reach)
+        landed(tok.at[array, slot(mask), side], tok_recv.at[array, side, reach - 1], TOKENS, array, side, reach)
+
+    def send_tok(array, side, number):
+        reach, step = ((0, 0), (0, 1), (0, 2), (1, 1), (1, 2), (2, 2), (3, 2))[number]
+        order = TOKEN_ORDERS[array][side]
+        if reach:
+            tok_landed(array, side, reach)
+        at = tok.at[array, slot(reached(order, reach)), side]
+        recv = tok_last.at[array] if step == 2 else tok_recv.at[array, side, (reach | 1 << step) - 1]
+        go(at, at, tok_send.at[0], recv, partner(order[step]))
 
     def tok_end(array):
-        for mask in range(1, n_slots):
-            tok_landed(array, mask)
+        for side in range(2):
+            for reach in (1, 2, 3):
+                tok_landed(array, side, reach)
+        landed(tok.at[array, : n_slots // 2], tok_last.at[array], TOKENS, array)
 
     sides = (UP, DOWN)
     source_of = (up_source, down_source)
@@ -236,19 +257,18 @@
             target = pass_of[kind] if which else slot_of[kind](core, place, pair)
             go(
                 source_of[kind](block(rep, 1 - pair, low_to)), target,
-                pair_send.at[which, kind], pair_recv.at[which, kind], partner(Y),
+                pair_send.at[0], pair_recv.at[kind], partner(Y),
             )
 
     def line_begin(kind):
         for step in steps:
             go(
                 source_of[kind](block(rep, pair, flip(low, step % 2))), slot_of[kind](core, place, pair),
-                line_send.at[step - 1, 0, kind], line_recv.at[step - 1, 0, kind], line_peer(step),
+                line_send.at[0], line_recv.at[step - 1, kind], line_peer(step),
             )
 
     def pair_end(kind):
-        landed(slot_of[kind](core, place, 1 - pair), pair_recv.at[0, kind], PAIR, kind, 0)
-        landed(pass_of[kind], pair_recv.at[1, kind], PAIR, kind, 1)
+        landed(slot_of[kind](core, place, 0, 2), pair_recv.at[kind], PAIR, kind)
 
     def line_pass(kind):
         pair_end(kind)
@@ -256,15 +276,11 @@
         for step in steps:
             go(
                 pass_of[kind] if step % 2 else near, near,
-                line_send.at[step - 1, 1, kind], line_recv.at[step - 1, 1, kind], line_peer(step),
+                line_send.at[0], line_recv.at[step - 1, kind], line_peer(step),
             )
 
     def line_landed(kind, step):
-        for number, pair_at in enumerate((pair, 1 - pair)):
-            landed(
-                slot_of[kind](core, place_at(step), pair_at), line_recv.at[step - 1, number, kind],
-                LINE, kind, step, number,
-            )
+        landed(slot_of[kind](core, place_at(step), 0, 2), line_recv.at[step - 1, kind], LINE, kind, step)
 
     def own_end(kind):
         pair_end(kind)
@@ -278,13 +294,11 @@
         else:
             own_end(kind)
         mine = slot_of[kind](core, place_at(step), 0, 2)
-        go(mine, mine, core_send.at[step, kind], core_recv.at[step, kind], other_core)
+        go(mine, mine, core_send.at[0], core_recv.at[kind], other_core)
 
     def weights_end(kind, number):
         if number:
-            for step in range(outer):
-                target = slot_of[kind](1 - core, place_at(step), 0, 2)
-                landed(target, core_recv.at[step, kind], CORE, kind, step)
+            landed((up_own, down_own)[kind].at[1 - core], core_recv.at[kind], CORE, kind)
         else:
             own_end(kind)
             for step in range(1, outer):
@@ -324,7 +338,7 @@
 
     def weight_grad(kind, half, columns):
         left = hidden[half] if kind == DOWN else pre_grad[half]
-        right = tok[COT if kind == DOWN else SAVED, :, :, columns].reshape(tokens, chunk)
+        right = tok[COT if kind == DOWN else SAVED, :, :, :, columns].reshape(tokens, chunk)
         return grad_scale * lax.dot_general(left, right, LEADING, preferred_element_type=jnp.float32)
 
     def grad_share(kind):
@@ -336,7 +350,7 @@
             columns = chunk_at(index)
             grad_sent[kind, :, columns] = weight_grad(kind, 1 - core, columns).astype(jnp.bfloat16)
 
-        go(grad_sent.at[kind], grad_got.at[kind], share_send.at[kind], share_recv.at[kind], other_core)
+        go(grad_sent.at[kind], grad_got.at[kind], share_send.at[0], share_recv.at[kind], other_core)
 
     def grad_keep(kind):
         if kind == DOWN:
@@ -362,28 +376,29 @@
                 columns = pl.ds(pl.multiple_of((place_at(step) * 2 + pair_at) * depth, depth), depth)
                 go(
                     grad_sum.at[kind, :, columns], grad_line.at[step - 1, kind, number],
-                    gline_send.at[step - 1, kind, number], gline_recv.at[step - 1, kind, number],
-                    line_peer(step),
+                    gline_send.at[0], gline_recv.at[kind, number], line_peer(step),
                 )
 
     def part_at(array, side, mask):
         return part.at[array, slot(mask), side]
 
+    def part_mask(array, side, number):
+        first, second, third = SUM_ORDERS[array][side]
+        return (second | third, second, third, 0, third, 0)[number]
+
     def part_first(array, side, number):
-        first, second = SUM_ORDERS[array][side]
+        first = SUM_ORDERS[array][side][0]
         for place_in in (2 * number, 2 * number + 1):
-            mask = (second | Z, second, Z, 0)[place_in]
             go(
-                part_at(array, side, first | mask), got_first.at[array, side, place_in],
-                part_send.at[array, side, place_in], part_recv.at[array, side, place_in], partner(first),
+                part_at(array, side, first | part_mask(array, side, place_in)),
+                got_first.at[array, side, place_in],
+                part_send.at[0], part_sem(array, side, place_in), partner(first),
             )
 
-    def part_landed(array, side, number):
-        got = got_first.at[array, side, number] if number < 4 else (
-            got_second.at[array, side, number - 4] if number < 6 else got_third.at[array, side]
-        )
-        landed(got, part_recv.at[array, side, number], PARTS, array, side, number)
-        return got
+    def part_sem(array, side, number):
+        if number in (3, 5, 6):
+            return part_end.at[array]
+        return part_recv.at[array, side, min(number, 2)]
 
     def part_add(array, side, mask, *got):
         total = part_at(array, side, mask)[...].astype(jnp.float32)
@@ -392,27 +407,33 @@
         return total
 
     def part_second(array, side, number):
-        first, second = SUM_ORDERS[array][side]
-        mask = (second | Z, second)[number]
-        got = part_landed(array, side, number)
+        mask = part_mask(array, side, number)
+        got = got_first.at[array, side, number]
+        landed(got, part_sem(array, side, number), SECOND, array, side, number)
         at = part_at(array, side, mask)
         at[...] = part_add(array, side, mask, got).astype(jnp.bfloat16)
         go(
             at, got_second.at[array, side, number],
-            part_send.at[array, side, 4 + number], part_recv.at[array, side, 4 + number], partner(second),
+            part_send.at[0], part_sem(array, side, 4 + number), partner(SUM_ORDERS[array][side][1]),
         )
 
     def part_third(array, side):
-        got = [part_landed(array, side, number) for number in (2, 4)]
-        at = part_at(array, side, Z)
-        at[...] = part_add(array, side, Z, *got).astype(jnp.bfloat16)
+        third = SUM_ORDERS[array][side][2]
+        got = (got_first.at[array, side, 2], got_second.at[array, side, 0])
+        landed(got_second.at[array, side], part_sem(array, side, 2), THIRD, array, side)
+        at = part_at(array, side, third)
+        at[...] = part_add(array, side, third, *got).astype(jnp.bfloat16)
         go(
             at, got_third.at[array, side],
-            part_send.at[array, side, 6], part_recv.at[array, side, 6], partner(Z),
+            part_send.at[0], part_sem(array, side, 6), partner(third),
         )
 
     def part_last(array, side):
-        return part_add(array, side, 0, *[part_landed(array, side, number) for number in (3, 5, 6)])
+        landed(part.at[array, : n_slots // 2 - 1], part_end.at[array], LAST, array, PARTS)
+        return part_add(
+            array, side, 0,
+            got_first.at[array, side, 3], got_second.at[array, side, 1], got_third.at[array, side],
+        )
 
     def back_sums():
         @pl.loop(0, outer)
@@ -460,11 +481,7 @@
         return grad_all.at[kind, pl.ds(block(rep_at, pair_at, 0), 2)]
 
     def grad_spread(kind, number):
-        for step in steps:
-            landed(
-                grad_line.at[step - 1, kind, number], gline_recv.at[step - 1, kind, number],
-                GRAD_LINE, kind, step, number,
-            )
+        landed(grad_line.at[:, kind, number], gline_recv.at[kind, number], GRAD_LINE, kind, number)
         for which, low_at in enumerate((low, 1 - low)):
             if number:
                 grad_all[kind, block(rep, pair, low_at)] = line_part(kind, which, number)
@@ -472,25 +489,34 @@
                 grad_pair[kind, low_at] = line_part(kind, which, number)
         mine = blocks_at(kind, rep, pair)
         if number:
-            go(mine, mine, grep_send.at[kind, 0], grep_recv.at[kind, 0], partner(X))
+            go(mine, mine, grep_send.at[0], grep_recv.at[kind, 0], partner(X))
             grad_out(kind, rep, pair)
         else:
-            go(grad_pair.at[kind], mine, gpair_send.at[kind], gpair_recv.at[kind], partner(Y))
+            go(grad_pair.at[kind], mine, gpair_send.at[0], gpair_recv.at[kind], partner(Y))
 
     def grad_pass(kind):
         near = blocks_at(kind, rep, 1 - pair)
         landed(near, gpair_recv.at[kind], GRAD_PAIR, kind)
-        go(near, near, grep_send.at[kind, 1], grep_recv.at[kind, 1], partner(X))
+        go(near, near, grep_send.at[0], grep_recv.at[kind, 1], partner(X))
         grad_out(kind, rep, 1 - pair)
 
+    def store(source, target, number):
+        pltpu.make_async_copy(source, target, store_sem.at[number]).start()
+
     def grad_out(kind, rep_at, pair_at):
+        if (ROWS, kind) not in seen:
+            seen.add((ROWS, kind))
+            sums[kind].wait()
         for low_at in range(2):
             index = block(rep_at, pair_at, low_at)
             place_to = pl.ds(pl.multiple_of(index * own, own), own)
             if kind == UP:
-                up_out[:, place_to] = grad_all[UP, index]
+                up_total[:, place_to] += grad_all[UP, index].astype(jnp.float32)
             else:
-                down_out[place_to, :] = grad_all[DOWN, index]
+                down_total[place_to, :] += grad_all[DOWN, index].astype(jnp.float32)
+        first = pl.ds(pl.multiple_of(block(rep_at, pair_at, 0) * own, own), 2 * own)
+        at = (slice(None), first) if kind == UP else (first, slice(None))
+        store((up_total, down_total)[kind].at[at], (up_out, down_out)[kind].at[at], kind)
 
     def grad_end(kind, number):
         pair_at = (pair, 1 - pair)[number]
@@ -499,7 +525,8 @@
 
     def share_rows(array):
         mine = rows_out.at[array, core]
-        go(mine, mine, out_send.at[array], out_recv.at[array], other_core)
+        go(mine, mine, out_send.at[0], out_recv.at[array], other_core)
+        store(mine, (input_out, mixed_out)[array].at[core], 2)
 
     def back_end():
         for side in range(2):
@@ -518,8 +545,8 @@
         share_rows(MIXED)
 
     def rows_end(array, out):
-        landed(rows_out.at[array, 1 - core], out_recv.at[array], ROWS, array)
-        out[...] = rows_out[array].reshape(2 * rows, width)
+        landed(rows_out.at[array, 1 - core], out_recv.at[array], LAST, array)
+        store(rows_out.at[array, 1 - core], out.at[1 - core], 2)
 
     def finish():
         for kind in KIND_ORDER:
@@ -527,8 +554,24 @@
                 grad_end(kind, number)
         rows_end(BACK, input_out)
         rows_end(MIXED, mixed_out)
-
-    for one in keep:
+        for number, whole in enumerate((up_total, down_total, rows_out)):
+            pltpu.make_async_copy(whole, whole, store_sem.at[number]).wait()
+        all_sent(tok.at[:, 1:], tok_send.at[0])
+        all_sent(part.at[:, 1:], part_send.at[0])
+        all_sent(up_own.at[:, : 3 * width // 4], line_send.at[0])
+        all_sent(grad_sum.at[:, :, : 3 * width // 4], gline_send.at[0])
+        all_sent(up_own.at[0, : width // 2], pair_send.at[0])
+        all_sent(up_own, core_send.at[0])
+        all_sent(grad_sent, share_send.at[0])
+        all_sent(grad_pair, gpair_send.at[0])
+        all_sent(grad_all.at[:, : n_fs // 2], grep_send.at[0])
+        all_sent(rows_out.at[:, 0], out_send.at[0])
+
+    sums = [
+        pltpu.make_async_copy(up_sum_ref, up_total, sum_sem.at[UP]),
+        pltpu.make_async_copy(down_sum_ref, down_total, sum_sem.at[DOWN]),
+    ]
+    for one in keep + sums:
         one.start()
     ends = (back_end, mixed_end)
     jobs = {
@@ -540,8 +583,18 @@
     }
     for job, *details in SCHEDULE:
         jobs[job](*details)
-    for one in sent:
-        one.wait_send()
+
+
+def store_kernel(*refs):
+    count = len(refs) // 2
+    copies = [
+        pltpu.make_async_copy(refs[index], refs[count + index], refs[-1].at[index])
+        for index in range(count)
+    ]
+    for one in copies:
+        one.start()
+    for one in copies:
+        one.wait()
 
 
 def cube_body(
@@ -558,20 +611,19 @@
     kind = x_later.dtype
     dma = pltpu.SemaphoreType.DMA
     vmem = functools.partial(pltpu.VMEM, dtype=kind)
-    inside = pl.BlockSpec(memory_space=pltpu.VMEM)
     outside = pl.BlockSpec(memory_space=pltpu.HBM)
-    mixed, input_gradient_rows, up_added, down_added = pl.pallas_call(
+    results = pl.pallas_call(
         functools.partial(layer_kernel, n_fs, grad_scale),
         out_shape=(
-            jax.ShapeDtypeStruct((row_count, width), kind),
-            jax.ShapeDtypeStruct((row_count, width), kind),
-            jax.ShapeDtypeStruct((depth, units), kind),
-            jax.ShapeDtypeStruct((units, depth), kind),
+            jax.ShapeDtypeStruct((2, 2, rows // 2, width), kind),
+            jax.ShapeDtypeStruct((2, 2, rows // 2, width), kind),
+            jax.ShapeDtypeStruct((depth, units), jnp.float32),
+            jax.ShapeDtypeStruct((units, depth), jnp.float32),
         ),
-        in_specs=[outside] * 3 + [inside] + [outside] * 2,
-        out_specs=[inside] * 4,
+        in_specs=[outside] * 8,
+        out_specs=[pl.BlockSpec(memory_space=pl.ANY)] * 4,
         scratch_shapes=[
-            vmem((rows, width)), vmem((rows, width)), vmem((3, n_fs, rows, width)),
+            pltpu.VMEM((1, width), jnp.float32), vmem((rows, width)), vmem((rows, width)), vmem((3, n_fs, 2, rows // 2, width)),
             vmem((2, width, own)), vmem((2, own, width)), vmem((depth, own)), vmem((own, depth)),
             pltpu.VMEM((2, tokens, own), jnp.float32), vmem((2, tokens, own)), vmem((2, tokens, own)),
             pltpu.VMEM((2, own, width), jnp.float32),
@@ -580,22 +632,33 @@
             vmem((2, n_fs, 2, rows // 2, width)),
             vmem((2, 2, 4, rows // 2, width)), vmem((2, 2, 2, rows // 2, width)),
             vmem((2, 2, rows // 2, width)), vmem((2, 2, 2, rows // 2, width)),
-            dma((3,)), dma((2, 2)), dma((2, 2)), dma((3, 2, 2)), dma((3, 2, 2)), dma((outer, 2)), dma((outer, 2)),
-            dma((2,)), dma((3, 7)), dma((3, 7)), dma((2,)), dma((2,)), dma((3, 2, 2)), dma((3, 2, 2)),
-            dma((2,)), dma((2,)), dma((2, 2)), dma((2, 2)), dma((2, 2, 7)), dma((2, 2, 7)), dma((2,)), dma((2,)),
+            pltpu.VMEM((depth, units), jnp.float32), pltpu.VMEM((units, depth), jnp.float32),
+            dma((5,)), dma((1,)), dma((2,)), dma((1,)), dma((3, 2)), dma((1,)), dma((2,)), dma((2,)),
+            dma((1,)), dma((3, 2, 3)), dma((3,)), dma((1,)), dma((2,)), dma((1,)), dma((2, 2)),
+            dma((1,)), dma((2,)), dma((1,)), dma((2, 2)), dma((1,)), dma((2, 2, 3)), dma((2,)),
+            dma((1,)), dma((2,)), dma((2,)), dma((3,)),
         ],
         compiler_params=pltpu.CompilerParams(
             collective_id=0, has_side_effects=True, vmem_limit_bytes=VMEM_BYTES
         ),
     )(
-        x_later, kept_input_rows, cotangent, norm_gain_vector.reshape(1, width), up_weight, down_weight,
-    )
-    return (
-        mixed,
-        input_gradient_rows,
-        up_sum + up_added.astype(jnp.float32),
-        down_sum + down_added.astype(jnp.float32),
-    )
+        *[
+            pltpu.with_memory_space_constraint(values, pltpu.HBM)
+            for values in (
+                x_later, kept_input_rows, cotangent, norm_gain_vector.reshape(1, width),
+                up_weight, down_weight, up_sum, down_sum,
+            )
+        ],
+    )
+    results = [one.reshape(row_count, width) for one in results[:2]] + list(results[2:])
+    return pl.pallas_call(
+        store_kernel,
+        out_shape=[jax.ShapeDtypeStruct(one.shape, one.dtype) for one in results],
+        in_specs=[pl.BlockSpec(memory_space=pl.ANY)] * len(results),
+        out_specs=[pl.BlockSpec(memory_space=pl.ANY)] * len(results),
+        scratch_shapes=[dma((len(results),))],
+        compiler_params=pltpu.CompilerParams(vmem_limit_bytes=2**20),
+    )(*results)
 
 
 def chosen_body(*args):

time: 136 us -> 124 us (0.912); the launches traced: 134 us -> 124 us
  other arithmetic: 5.22 us -> 0 us
  Pallas kernels: 127 us -> 123 us
  local copies, waits for them, and re-layouts: 1.6 us -> 0 us
    pallas_call x1, Pallas kernels: 127 us -> 121 us  [cube_body(): pl.pallas_call(functools.partial(layer_kernel, n_fs, grad_scale), out_sha...]
    add x2 -> x0, other arithmetic: 5.22 us -> none  [the longest x1 3.7 us: cube_body(): up_sum + up_added.astype(jnp.float32)]
    pallas_call x0 -> x1, Pallas kernels: none -> 2.39 us  [cube_body(): pl.pallas_call(store_kernel, out_shape=[jax.ShapeDtypeStruct(one.shape, o...]
    unnamed x10 -> x0, local copies, waits for them, and re-layouts: 1.6 us -> none
where the time goes in v3:
time: 124 us
  Pallas kernels  123 us (99%)
    pallas_call x1, Pallas kernels, cube_body(): pl.pallas_call(functools.partial(layer_kernel, n_fs, grad_scale), out_sha...  121 us

profile of v3, /device:TPU:0, one launch (start us, length us, event | category | flops | bytes accessed | tf_op | source)
XLA Modules:
  0.0 124.0 jit_solution(14668761413153098476)
XLA Ops:
  0.6 121.0 %shard_map.111 = (bf16[2,2,32,2048]{3,2,1,0:T(8,128)(2,1)S(1)}, bf16[2,2,32,2048]{3,2,1,0:T(8,128)(2,1)S(1)}, f32[256,2048]{1,0:T(8,128)S(1)}, f32[2048,256]{1,0:T(8,128)S(1)}) custom-call(bf16[128,2048]{1,0:T(8,128)(2,1)} %x_ref.1, bf16[128,2048]{1,0:T(8,128)(2,1)} %kept_ref.1, bf16[128,2048]{1,0:T(8,128)(2,1)} %cot_ref.1, f32[1,2048]{1,0:T(1,128)} %bitcast.5, ...), custom_call_target="tpu_custom_call" | custom-call | tf_op jit(solution)/shard_map/pallas_call | solution.py:615
  121.7 2.4 %shard_map.112 = (bf16[128,2048]{1,0:T(8,128)(2,1)}, bf16[128,2048]{1,0:T(8,128)(2,1)}, f32[256,2048]{1,0:T(8,128)}, f32[2048,256]{1,0:T(8,128)}) custom-call(bf16[128,2048]{1,0:T(8,128)(2,1)S(1)} %bitcast.3, bf16[128,2048]{1,0:T(8,128)(2,1)S(1)} %bitcast.4, f32[256,2048]{1,0:T(8,128)S(1)} %get-tuple-element.10.refs_2_, ...), custom_call_target="tpu_custom_call" | custom-call | tf_op jit(solution)/shard_map/pallas_call | solution.py:654

commit v4 on v3

--- a/solution.py
+++ b/solution.py
@@ -16,31 +16,37 @@
 BACK, MIXED = 0, 1
 UP, DOWN = 0, 1
 (TOK, PAIR, LINE, LINE_PASS, CORE, PRE, GRAD, SHARE, KEEP, GRAD_LINE,
- GRAD_PAIR, GRAD_REP, BACK_SUMS, MIXED_SUMS, FIRST, SECOND, THIRD, LAST, END, TOKENS, OWN, PARTS, ROWS) = range(23)
+ GRAD_PAIR, GRAD_REP, BACK_SUMS, MIXED_SUMS, FIRST, SECOND, THIRD, LAST, END, GRAD_GO, TOKENS, OWN, PARTS, ROWS) = range(24)
 KIND_ORDER = (DOWN, UP)
-TOKEN_ORDERS = (((Z, X, Y), (Z, Y, X)), ((Z, Y, X), (Z, Y, X)), ((Z, X, Y), (Z, Y, X)))
-SUM_ORDERS = (((Y, X, Z), (X, Y, Z)), ((Y, X, Z), (Y, X, Z)))
+TOKEN_ORDERS = (((Z, Y, X), (Z, X, Y)), ((Z, Y, X), (Z, Y, X)), ((Z, Y, X), (Z, X, Y)))
+SUM_ORDERS = (((Y, X, Z), (X, Z, Y)), ((Y, X, Z), (Y, Z, X)))
 SCHEDULE = (
-    (TOK, COT, 1, 1), (TOK, COT, 0, 0), (TOK, COT, 0, 1), (TOK, SAVED, 0, 2), (TOK, SAVED, 1, 1),
-    (TOK, SAVED, 1, 0), (TOK, LATER, 0, 1), (LINE, UP), (TOK, LATER, 1, 1), (TOK, COT, 1, 5),
-    (TOK, SAVED, 1, 2), (PAIR, UP), (TOK, COT, 1, 2), (TOK, SAVED, 0, 0), (CORE, UP, 0),
-    (TOK, COT, 1, 0), (TOK, SAVED, 0, 1), (TOK, LATER, 0, 0), (LINE_PASS, UP), (TOK, LATER, 1, 5),
-    (TOK, SAVED, 0, 3), (TOK, COT, 0, 4), (LINE, DOWN), (TOK, SAVED, 1, 4), (TOK, SAVED, 1, 3),
-    (TOK, LATER, 1, 0), (TOK, COT, 0, 3), (TOK, COT, 0, 5), (TOK, SAVED, 0, 5), (TOK, SAVED, 1, 5),
-    (PAIR, DOWN), (TOK, COT, 1, 3), (TOK, SAVED, 1, 6), (TOK, SAVED, 0, 4), (CORE, UP, 2),
-    (TOK, COT, 0, 2), (CORE, UP, 1), (TOK, SAVED, 0, 6), (TOK, COT, 0, 6), (CORE, UP, 3),
-    (TOK, COT, 1, 6), (CORE, DOWN, 0), (TOK, COT, 1, 4), (TOK, LATER, 0, 4), (LINE_PASS, DOWN),
-    (TOK, LATER, 0, 5), (TOK, LATER, 1, 3), (TOK, LATER, 1, 2), (TOK, LATER, 0, 2), (PRE, 1),
-    (PRE, 0), (SHARE, DOWN), (TOK, LATER, 0, 3), (TOK, LATER, 1, 4), (KEEP, DOWN),
-    (GRAD_LINE, DOWN), (CORE, DOWN, 1), (CORE, DOWN, 3), (TOK, LATER, 0, 6), (CORE, DOWN, 2),
-    (GRAD, 0), (TOK, LATER, 1, 6), (GRAD, 1), (BACK_SUMS,), (FIRST, BACK, 1, 1),
-    (FIRST, BACK, 0, 1), (KEEP, UP), (SHARE, UP), (FIRST, BACK, 1, 0), (FIRST, BACK, 0, 0),
-    (SECOND, BACK, 0, 0), (GRAD_PAIR, DOWN, 0), (SECOND, BACK, 0, 1), (MIXED_SUMS,),
-    (FIRST, MIXED, 0, 0), (GRAD_LINE, UP), (FIRST, MIXED, 0, 1), (GRAD_PAIR, DOWN, 1),
-    (FIRST, MIXED, 1, 0), (GRAD_REP, DOWN), (SECOND, MIXED, 0, 1), (SECOND, BACK, 1, 0),
-    (SECOND, MIXED, 1, 0), (SECOND, MIXED, 0, 0), (GRAD_PAIR, UP, 0), (SECOND, MIXED, 1, 1),
-    (THIRD, BACK, 1), (GRAD_PAIR, UP, 1), (THIRD, BACK, 0), (FIRST, MIXED, 1, 1), (THIRD, MIXED, 0),
-    (GRAD_REP, UP), (THIRD, MIXED, 1), (SECOND, BACK, 1, 1), (LAST, MIXED), (LAST, BACK), (END,),
+    (TOK, COT, 0, 2), (TOK, SAVED, 1, 1), (TOK, COT, 1, 1), (TOK, COT, 0, 1), (TOK, SAVED, 1, 2),
+    (LINE, DOWN, 2), (PAIR, UP), (TOK, COT, 1, 0), (PAIR, DOWN), (TOK, SAVED, 1, 5),
+    (TOK, LATER, 1, 1), (TOK, SAVED, 0, 0), (TOK, COT, 1, 5), (LINE, UP, 2), (TOK, COT, 1, 3),
+    (TOK, SAVED, 0, 1), (TOK, LATER, 1, 2), (TOK, SAVED, 1, 0), (LINE_PASS, UP, 3),
+    (TOK, COT, 0, 0), (TOK, COT, 0, 5), (TOK, SAVED, 0, 4), (TOK, SAVED, 1, 3), (TOK, SAVED, 1, 4),
+    (TOK, COT, 1, 6), (TOK, SAVED, 0, 3), (LINE, UP, 1), (LINE_PASS, UP, 2), (CORE, DOWN, 0),
+    (LINE_PASS, UP, 1), (TOK, SAVED, 0, 2), (LINE_PASS, DOWN, 2), (TOK, LATER, 1, 0),
+    (TOK, SAVED, 1, 6), (LINE, UP, 3), (TOK, COT, 0, 4), (TOK, COT, 0, 3), (TOK, COT, 1, 2),
+    (TOK, LATER, 0, 0), (TOK, SAVED, 0, 5), (TOK, SAVED, 0, 6), (TOK, COT, 1, 4), (TOK, COT, 0, 6),
+    (TOK, LATER, 1, 5), (LINE_PASS, DOWN, 1), (CORE, UP, 2), (LINE, DOWN, 3), (TOK, LATER, 1, 3),
+    (TOK, LATER, 0, 3), (CORE, UP, 0), (CORE, UP, 3), (TOK, LATER, 0, 1), (TOK, LATER, 1, 4),
+    (CORE, UP, 1), (PRE, 0), (LINE, DOWN, 1), (CORE, DOWN, 2), (LINE_PASS, DOWN, 3), (PRE, 1),
+    (SHARE, DOWN), (TOK, LATER, 0, 4), (KEEP, DOWN), (TOK, LATER, 0, 2), (GRAD_LINE, DOWN),
+    (GRAD_GO, DOWN, 0, 2), (TOK, LATER, 0, 6), (GRAD_GO, DOWN, 0, 1), (CORE, DOWN, 1),
+    (GRAD_GO, DOWN, 0, 3), (TOK, LATER, 1, 6), (CORE, DOWN, 3), (GRAD_GO, DOWN, 1, 1), (GRAD, 0),
+    (TOK, LATER, 0, 5), (GRAD, 1), (BACK_SUMS, 0), (FIRST, BACK, 0, 0), (BACK_SUMS, 1),
+    (FIRST, BACK, 1, 1), (MIXED_SUMS, 1), (FIRST, MIXED, 1, 0), (GRAD_GO, DOWN, 1, 2),
+    (FIRST, BACK, 1, 0), (MIXED_SUMS, 0), (SHARE, UP), (KEEP, UP), (GRAD_LINE, UP),
+    (GRAD_GO, UP, 0, 1), (SECOND, MIXED, 1, 0), (FIRST, MIXED, 0, 0), (GRAD_GO, UP, 0, 3),
+    (GRAD_GO, UP, 1, 1), (GRAD_PAIR, DOWN, 0), (GRAD_GO, UP, 0, 2), (SECOND, BACK, 0, 0),
+    (SECOND, BACK, 0, 1), (GRAD_GO, DOWN, 1, 3), (SECOND, MIXED, 0, 0), (FIRST, MIXED, 1, 1),
+    (SECOND, MIXED, 0, 1), (GRAD_REP, DOWN), (GRAD_PAIR, UP, 0), (GRAD_GO, UP, 1, 3),
+    (SECOND, BACK, 1, 0), (FIRST, MIXED, 0, 1), (THIRD, MIXED, 1), (GRAD_PAIR, DOWN, 1),
+    (SECOND, BACK, 1, 1), (GRAD_GO, UP, 1, 2), (GRAD_REP, UP), (SECOND, MIXED, 1, 1),
+    (THIRD, MIXED, 0), (FIRST, BACK, 0, 1), (GRAD_PAIR, UP, 1), (THIRD, BACK, 1), (THIRD, BACK, 0),
+    (LAST, MIXED), (LAST, BACK), (END,),
 )
 VMEM_BYTES = 48 * 2**20
 
@@ -237,20 +243,19 @@
         if reach:
             tok_landed(array, side, reach)
         at = tok.at[array, slot(reached(order, reach)), side]
-        recv = tok_last.at[array] if step == 2 else tok_recv.at[array, side, (reach | 1 << step) - 1]
+        recv = tok_last.at[array, side] if step == 2 else tok_recv.at[array, side, (reach | 1 << step) - 1]
         go(at, at, tok_send.at[0], recv, partner(order[step]))
 
-    def tok_end(array):
-        for side in range(2):
+    def tok_end(array, which=(0, 1)):
+        for side in which:
             for reach in (1, 2, 3):
                 tok_landed(array, side, reach)
-        landed(tok.at[array, : n_slots // 2], tok_last.at[array], TOKENS, array)
+            landed(tok.at[array, : n_slots // 2, side], tok_last.at[array, side], TOKENS, array, side)
 
     sides = (UP, DOWN)
     source_of = (up_source, down_source)
     slot_of = (up_slot, down_slot)
     pass_of = (up_pass, down_pass)
-    steps = (1, 3, 2)
 
     def pair_begin(kind):
         for which, low_to in enumerate((low, 1 - low)):
@@ -260,24 +265,22 @@
                 pair_send.at[0], pair_recv.at[kind], partner(Y),
             )
 
-    def line_begin(kind):
-        for step in steps:
-            go(
-                source_of[kind](block(rep, pair, flip(low, step % 2))), slot_of[kind](core, place, pair),
-                line_send.at[0], line_recv.at[step - 1, kind], line_peer(step),
-            )
+    def line_begin(kind, step):
+        go(
+            source_of[kind](block(rep, pair, flip(low, step % 2))), slot_of[kind](core, place, pair),
+            line_send.at[0], line_recv.at[step - 1, kind], line_peer(step),
+        )
 
     def pair_end(kind):
         landed(slot_of[kind](core, place, 0, 2), pair_recv.at[kind], PAIR, kind)
 
-    def line_pass(kind):
+    def line_pass(kind, step):
         pair_end(kind)
         near = slot_of[kind](core, place, 1 - pair)
-        for step in steps:
-            go(
-                pass_of[kind] if step % 2 else near, near,
-                line_send.at[0], line_recv.at[step - 1, kind], line_peer(step),
-            )
+        go(
+            pass_of[kind] if step % 2 else near, near,
+            line_send.at[0], line_recv.at[step - 1, kind], line_peer(step),
+        )
 
     def line_landed(kind, step):
         landed(slot_of[kind](core, place_at(step), 0, 2), line_recv.at[step - 1, kind], LINE, kind, step)
@@ -320,7 +323,7 @@
         weights_end(UP, number)
         pre = jnp.dot(all_tokens(SAVED), up_own[half], preferred_element_type=jnp.float32)
         pre_kept[half] = jax.nn.relu(pre)
-        hidden[half] = squared_relu(pre)
+        hidden[half] = squared_relu(pre).reshape(hidden.shape[1:])
 
     def saved_grad(number):
         half = (core, 1 - core)[number]
@@ -329,7 +332,7 @@
         grad = lax.dot_general(
             all_tokens(COT), down_own[half], TRANSPOSED, preferred_element_type=jnp.float32
         )
-        pre_grad[half] = (grad * 2.0 * pre_kept[half]).astype(jnp.bfloat16)
+        pre_grad[half] = (grad * 2.0 * pre_kept[half]).astype(jnp.bfloat16).reshape(pre_grad.shape[1:])
 
     chunk = width // outer
 
@@ -337,7 +340,7 @@
         return pl.ds(pl.multiple_of(index * chunk, chunk), chunk)
 
     def weight_grad(kind, half, columns):
-        left = hidden[half] if kind == DOWN else pre_grad[half]
+        left = (hidden[half] if kind == DOWN else pre_grad[half]).reshape(tokens, own)
         right = tok[COT if kind == DOWN else SAVED, :, :, :, columns].reshape(tokens, chunk)
         return grad_scale * lax.dot_general(left, right, LEADING, preferred_element_type=jnp.float32)
 
@@ -371,13 +374,13 @@
                 grad_kept[kind, :, columns] + grad_got[kind, :, columns].astype(jnp.float32)
             ).astype(jnp.bfloat16)
 
-        for number, pair_at in enumerate((1 - pair, pair)):
-            for step in steps:
-                columns = pl.ds(pl.multiple_of((place_at(step) * 2 + pair_at) * depth, depth), depth)
-                go(
-                    grad_sum.at[kind, :, columns], grad_line.at[step - 1, kind, number],
-                    gline_send.at[0], gline_recv.at[kind, number], line_peer(step),
-                )
+    def grad_go(kind, number, step):
+        pair_at = (1 - pair, pair)[number]
+        columns = pl.ds(pl.multiple_of((place_at(step) * 2 + pair_at) * depth, depth), depth)
+        go(
+            grad_sum.at[kind, :, columns], grad_line.at[step - 1, kind, number],
+            gline_send.at[0], gline_recv.at[kind, number], line_peer(step),
+        )
 
     def part_at(array, side, mask):
         return part.at[array, slot(mask), side]
@@ -435,36 +438,45 @@
             got_first.at[array, side, 3], got_second.at[array, side, 1], got_third.at[array, side],
         )
 
-    def back_sums():
+    def side_of(ref, side):
+        return ref[:, side].reshape(tokens // 2, ref.shape[-1])
+
+    def store_part(array, side, columns, total):
+        part[array, :, side, :, columns] = total.astype(jnp.bfloat16).reshape(n_slots, half_rows, chunk)
+
+    def back_sums(side):
         @pl.loop(0, outer)
         def _(index):
             columns = chunk_at(index)
-            total = jnp.zeros((tokens, chunk), jnp.float32)
+            total = jnp.zeros((tokens // 2, chunk), jnp.float32)
             for half in range(2):
                 total = total + lax.dot_general(
-                    pre_grad[half], up_own[half, columns, :], TRANSPOSED,
+                    side_of(pre_grad.at[half], side), up_own[half, columns, :], TRANSPOSED,
                     preferred_element_type=jnp.float32,
                 )
-            part[BACK, :, :, :, columns] = total.astype(jnp.bfloat16).reshape(n_slots, 2, rows // 2, chunk)
-
-    def mixed_sums():
-        tok_end(LATER)
+            store_part(BACK, side, columns, total)
+
+    def mixed_sums(side):
+        tok_end(LATER, (side,))
 
         @pl.loop(0, 2)
         def _(half):
-            hidden[half] = squared_relu(
-                jnp.dot(all_tokens(LATER), up_own[half], preferred_element_type=jnp.float32)
-            )
+            hidden[half, :, side] = squared_relu(
+                jnp.dot(
+                    side_of(tok.at[LATER], side), up_own[half], preferred_element_type=jnp.float32
+                )
+            ).reshape(n_slots, half_rows, own)
 
         @pl.loop(0, outer)
         def _(index):
             columns = chunk_at(index)
-            total = jnp.zeros((tokens, chunk), jnp.float32)
+            total = jnp.zeros((tokens // 2, chunk), jnp.float32)
             for half in range(2):
                 total = total + jnp.dot(
-                    hidden[half], down_own[half, :, columns], preferred_element_type=jnp.float32
+                    side_of(hidden.at[half], side), down_own[half, :, columns],
+                    preferred_element_type=jnp.float32,
                 )
-            part[MIXED, :, :, :, columns] = total.astype(jnp.bfloat16).reshape(n_slots, 2, rows // 2, chunk)
+            store_part(MIXED, side, columns, total)
 
     def line_part(kind, which, number):
         if which:
@@ -576,7 +588,7 @@
     ends = (back_end, mixed_end)
     jobs = {
         TOK: send_tok, PAIR: pair_begin, LINE: line_begin, LINE_PASS: line_pass, CORE: to_core,
-        PRE: saved_pre, GRAD: saved_grad, SHARE: grad_share, KEEP: grad_keep, GRAD_LINE: grad_begin,
+        PRE: saved_pre, GRAD: saved_grad, SHARE: grad_share, KEEP: grad_keep, GRAD_LINE: grad_begin, GRAD_GO: grad_go,
         GRAD_PAIR: grad_spread, GRAD_REP: grad_pass, BACK_SUMS: back_sums, MIXED_SUMS: mixed_sums,
         FIRST: part_first, SECOND: part_second, THIRD: part_third, LAST: lambda array: ends[array](),
         END: finish,
@@ -625,7 +637,7 @@
         scratch_shapes=[
             pltpu.VMEM((1, width), jnp.float32), vmem((rows, width)), vmem((rows, width)), vmem((3, n_fs, 2, rows // 2, width)),
             vmem((2, width, own)), vmem((2, own, width)), vmem((depth, own)), vmem((own, depth)),
-            pltpu.VMEM((2, tokens, own), jnp.float32), vmem((2, tokens, own)), vmem((2, tokens, own)),
+            pltpu.VMEM((2, tokens, own), jnp.float32), vmem((2, n_fs, 2, rows // 2, own)), vmem((2, n_fs, 2, rows // 2, own)),
             pltpu.VMEM((2, own, width), jnp.float32),
             vmem((2, own, width)), vmem((2, own, width)), vmem((2, own, width)),
             vmem((3, 2, 2, own, depth)), vmem((2, 2, own, depth)), vmem((2, n_fs, own, depth)),
@@ -634,7 +646,7 @@
             vmem((2, 2, rows // 2, width)), vmem((2, 2, 2, rows // 2, width)),
             pltpu.VMEM((depth, units), jnp.float32), pltpu.VMEM((units, depth), jnp.float32),
             dma((5,)), dma((1,)), dma((2,)), dma((1,)), dma((3, 2)), dma((1,)), dma((2,)), dma((2,)),
-            dma((1,)), dma((3, 2, 3)), dma((3,)), dma((1,)), dma((2,)), dma((1,)), dma((2, 2)),
+            dma((1,)), dma((3, 2, 3)), dma((3, 2)), dma((1,)), dma((2,)), dma((1,)), dma((2, 2)),
             dma((1,)), dma((2,)), dma((1,)), dma((2, 2)), dma((1,)), dma((2, 2, 3)), dma((2,)),
             dma((1,)), dma((2,)), dma((2,)), dma((3,)),
         ],

time: 124 us -> 119 us (0.960)
  Pallas kernels: 123 us -> 119 us
    pallas_call x1, Pallas kernels: 121 us -> 116 us  [cube_body(): pl.pallas_call(functools.partial(layer_kernel, n_fs, grad_scale), out_sha...]
where the time goes in v4:
time: 119 us
  Pallas kernels  119 us (100%)
    pallas_call x1, Pallas kernels, cube_body(): pl.pallas_call(functools.partial(layer_kernel, n_fs, grad_scale), out_sha...  116 us
    pallas_call x1, Pallas kernels, cube_body(): pl.pallas_call(store_kernel, out_shape=[jax.ShapeDtypeStruct(one.shape, o...  2.39 us

profile of v4, /device:TPU:0, one launch (start us, length us, event | category | flops | bytes accessed | tf_op | source)
XLA Modules:
  0.0 119.2 jit_solution(18393223586302585609)
XLA Ops:
  0.6 116.2 %shard_map.111 = (bf16[2,2,32,2048]{3,2,1,0:T(8,128)(2,1)S(1)}, bf16[2,2,32,2048]{3,2,1,0:T(8,128)(2,1)S(1)}, f32[256,2048]{1,0:T(8,128)S(1)}, f32[2048,256]{1,0:T(8,128)S(1)}) custom-call(bf16[128,2048]{1,0:T(8,128)(2,1)} %x_ref.1, bf16[128,2048]{1,0:T(8,128)(2,1)} %kept_ref.1, bf16[128,2048]{1,0:T(8,128)(2,1)} %cot_ref.1, f32[1,2048]{1,0:T(1,128)} %bitcast.5, ...), custom_call_target="tpu_custom_call" | custom-call | tf_op jit(solution)/shard_map/pallas_call | solution.py:627
  116.8 2.4 %shard_map.112 = (bf16[128,2048]{1,0:T(8,128)(2,1)}, bf16[128,2048]{1,0:T(8,128)(2,1)}, f32[256,2048]{1,0:T(8,128)}, f32[2048,256]{1,0:T(8,128)}) custom-call(bf16[128,2048]{1,0:T(8,128)(2,1)S(1)} %bitcast.3, bf16[128,2048]{1,0:T(8,128)(2,1)S(1)} %bitcast.4, f32[256,2048]{1,0:T(8,128)S(1)} %get-tuple-element.10.refs_2_, ...), custom_call_target="tpu_custom_call" | custom-call | tf_op jit(solution)/shard_map/pallas_call | solution.py:666

commit v5 on v4

--- a/solution.py
+++ b/solution.py
@@ -190,13 +190,17 @@
             copy(target, target, sem, sem, other_core).wait_recv()
 
     own_rows = pl.ds(start_row, rows)
+
+    def own_half(side):
+        return pl.ds(pl.multiple_of(start_row + side * half_rows, half_rows), half_rows)
+
     loads = [
         pltpu.make_async_copy(kept_ref.at[own_rows, :], kept, load_sem.at[0]),
         pltpu.make_async_copy(x_ref.at[own_rows, :], fresh, load_sem.at[1]),
     ]
     loads += [
         pltpu.make_async_copy(
-            cot_ref.at[pl.ds(pl.multiple_of(start_row + side * half_rows, half_rows), half_rows), :],
+            cot_ref.at[own_half(side), :],
             tok.at[COT, slot(0), side], load_sem.at[2 + side],
         )
         for side in range(2)
@@ -211,13 +215,22 @@
     for peer in peers:
         pl.semaphore_signal(barrier, inc=1, device_id=peer, device_id_type=MESH)
 
-    for one in loads:
-        one.wait()
-    gain = gain_kept[...]
-    own_shape = (2, half_rows, width)
-    tok[SAVED, slot(0)] = norm_partial_terms(kept[...], gain)[2].reshape(own_shape)
-    tok[LATER, slot(0)] = norm_partial_terms(fresh[...], gain)[2].reshape(own_shape)
     pl.semaphore_wait(barrier, len(peers))
+
+    def own_ready(array):
+        if (OWN, array, TOK) in seen:
+            return
+        seen.add((OWN, array, TOK))
+        if array == COT:
+            loads[2].wait()
+            loads[3].wait()
+            return
+        if OWN not in seen:
+            seen.add(OWN)
+            loads[4].wait()
+        loads[array == LATER].wait()
+        normed = norm_partial_terms((kept if array == SAVED else fresh)[...], gain_kept[...])[2]
+        tok[array, slot(0)] = normed.reshape(2, half_rows, width)
 
     def up_source(index):
         return up_ref.at[:, pl.ds(pl.multiple_of(index * own, own), own)]
@@ -243,10 +256,16 @@
         if reach:
             tok_landed(array, side, reach)
         at = tok.at[array, slot(reached(order, reach)), side]
+        source = at
+        if not reach and array == COT:
+            source = cot_ref.at[own_half(side), :]
+        elif not reach:
+            own_ready(array)
         recv = tok_last.at[array, side] if step == 2 else tok_recv.at[array, side, (reach | 1 << step) - 1]
-        go(at, at, tok_send.at[0], recv, partner(order[step]))
+        go(source, at, tok_send.at[0], recv, partner(order[step]))
 
     def tok_end(array, which=(0, 1)):
+        own_ready(array)
         for side in which:
             for reach in (1, 2, 3):
                 tok_landed(array, side, reach)
@@ -542,9 +561,9 @@
 
     def back_end():
         for side in range(2):
-            scaled_rows = part_last(BACK, side) * gain
+            scaled_rows = part_last(BACK, side) * gain_kept[...]
             at = pl.ds(side * (rows // 2), rows // 2)
-            inverse, unit_rows, _ = norm_partial_terms(kept[at, :], gain)
+            inverse, unit_rows, _ = norm_partial_terms(kept[at, :], gain_kept[...])
             rows_out[BACK, core, side] = (
                 inverse
                 * (scaled_rows - unit_rows * jnp.mean(scaled_rows * unit_rows, axis=-1, keepdims=True))

time: 119 us -> 119 us (level)
  no operation moved by 1% of the time
where the time goes in v5:
time: 119 us
  Pallas kernels  118 us (99%)
    pallas_call x1, Pallas kernels, cube_body(): pl.pallas_call(functools.partial(layer_kernel, n_fs, grad_scale), out_sha...  116 us
    pallas_call x1, Pallas kernels, cube_body(): pl.pallas_call(store_kernel, out_shape=[jax.ShapeDtypeStruct(one.shape, o...  2.39 us

profile of v5, /device:TPU:0, one launch (start us, length us, event | category | flops | bytes accessed | tf_op | source)
XLA Modules:
  0.0 118.6 jit_solution(18159807908206970187)
XLA Ops:
  0.6 115.6 %shard_map.111 = (bf16[2,2,32,2048]{3,2,1,0:T(8,128)(2,1)S(1)}, bf16[2,2,32,2048]{3,2,1,0:T(8,128)(2,1)S(1)}, f32[256,2048]{1,0:T(8,128)S(1)}, f32[2048,256]{1,0:T(8,128)S(1)}) custom-call(bf16[128,2048]{1,0:T(8,128)(2,1)} %x_ref.1, bf16[128,2048]{1,0:T(8,128)(2,1)} %kept_ref.1, bf16[128,2048]{1,0:T(8,128)(2,1)} %cot_ref.1, f32[1,2048]{1,0:T(1,128)} %bitcast.5, ...), custom_call_target="tpu_custom_call" | custom-call | tf_op jit(solution)/shard_map/pallas_call | solution.py:646
  116.2 2.4 %shard_map.112 = (bf16[128,2048]{1,0:T(8,128)(2,1)}, bf16[128,2048]{1,0:T(8,128)(2,1)}, f32[256,2048]{1,0:T(8,128)}, f32[2048,256]{1,0:T(8,128)}) custom-call(bf16[128,2048]{1,0:T(8,128)(2,1)S(1)} %bitcast.3, bf16[128,2048]{1,0:T(8,128)(2,1)S(1)} %bitcast.4, f32[256,2048]{1,0:T(8,128)S(1)} %get-tuple-element.10.refs_2_, ...), custom_call_target="tpu_custom_call" | custom-call | tf_op jit(solution)/shard_map/pallas_call | solution.py:685

commit v6 on v5

--- a/solution.py
+++ b/solution.py
@@ -580,11 +580,13 @@
         store(rows_out.at[array, 1 - core], out.at[1 - core], 2)
 
     def finish():
-        for kind in KIND_ORDER:
-            for number in range(2):
-                grad_end(kind, number)
+        first, last = KIND_ORDER
+        grad_end(first, 0)
+        grad_end(first, 1)
+        grad_end(last, 1)
         rows_end(BACK, input_out)
         rows_end(MIXED, mixed_out)
+        grad_end(last, 0)
         for number, whole in enumerate((up_total, down_total, rows_out)):
             pltpu.make_async_copy(whole, whole, store_sem.at[number]).wait()
         all_sent(tok.at[:, 1:], tok_send.at[0])

time: 119 us -> 119 us (level)
  no operation moved by 1% of the time
where the time goes in v6:
time: 119 us; the launch traced here: 118 us
  Pallas kernels  118 us (99%)
    pallas_call x1, Pallas kernels, cube_body(): pl.pallas_call(functools.partial(layer_kernel, n_fs, grad_scale), out_sha...  115 us
    pallas_call x1, Pallas kernels, cube_body(): pl.pallas_call(store_kernel, out_shape=[jax.ShapeDtypeStruct(one.shape, o...  2.39 us

profile of v6, /device:TPU:0, one launch (start us, length us, event | category | flops | bytes accessed | tf_op | source)
XLA Modules:
  0.0 118.5 jit_solution(4959804671201888700)
XLA Ops:
  0.6 115.4 %shard_map.111 = (bf16[2,2,32,2048]{3,2,1,0:T(8,128)(2,1)S(1)}, bf16[2,2,32,2048]{3,2,1,0:T(8,128)(2,1)S(1)}, f32[256,2048]{1,0:T(8,128)S(1)}, f32[2048,256]{1,0:T(8,128)S(1)}) custom-call(bf16[128,2048]{1,0:T(8,128)(2,1)} %x_ref.1, bf16[128,2048]{1,0:T(8,128)(2,1)} %kept_ref.1, bf16[128,2048]{1,0:T(8,128)(2,1)} %cot_ref.1, f32[1,2048]{1,0:T(1,128)} %bitcast.5, ...), custom_call_target="tpu_custom_call" | custom-call | tf_op jit(solution)/shard_map/pallas_call | solution.py:648
  116.1 2.4 %shard_map.112 = (bf16[128,2048]{1,0:T(8,128)(2,1)}, bf16[128,2048]{1,0:T(8,128)(2,1)}, f32[256,2048]{1,0:T(8,128)}, f32[2048,256]{1,0:T(8,128)}) custom-call(bf16[128,2048]{1,0:T(8,128)(2,1)S(1)} %bitcast.3, bf16[128,2048]{1,0:T(8,128)(2,1)S(1)} %bitcast.4, f32[256,2048]{1,0:T(8,128)S(1)} %get-tuple-element.10.refs_2_, ...), custom_call_target="tpu_custom_call" | custom-call | tf_op jit(solution)/shard_map/pallas_call | solution.py:687
